TPU v7x, 512 devices: a whole 4x4x16 slice. The times are simulated.
512 devices in a mesh: kv: 16 (over y, x), tp: 32 (over z, core).
Axes of the slice: x: 4, y: 4, z: 16, core: 2. Of those that a mesh axis runs over, the one named last changes fastest.
Arguments:
- tokens: bfloat16 [16, 4096], P(None, ('kv', 'tp')), may hold values from -8 to 8
- attention_gain: bfloat16 [4096], replicated, may hold values from 0.099609375 to 1.8984375
- query_weight: bfloat16 [2048, 4096], P('tp', 'kv'), may hold values from -0.09375 to 0.09375
- key_weight: bfloat16 [2048, 4096], P('tp', 'kv'), may hold values from -0.09375 to 0.09375
- value_weight: bfloat16 [2048, 4096], P('tp', 'kv'), may hold values from -0.09375 to 0.09375
- forget_weight: bfloat16 [32, 4096], replicated, may hold values from -0.09375 to 0.09375
- cached_pairs: bfloat16 [16, 32, 2, 64, 16384], P(None, 'tp', None, None, 'kv'), may hold values from -200 to 200
- cached_gates: float32 [16, 32, 16384], P(None, 'tp', 'kv'), as said below
- lengths: int32 [16], replicated, may hold values from 1 to 16384, as said below
- output_weight: bfloat16 [2048, 4096], P('tp', 'kv'), may hold values from -1.5 to 1.5
- mixer_gain: bfloat16 [4096], replicated, may hold values from 0.099609375 to 1.8984375
- up_weight: bfloat16 [16384, 4096], P('tp', 'kv'), may hold values from -0.09375 to 0.09375
- down_weight: bfloat16 [16384, 4096], P('tp', 'kv'), may hold values from -0.09375 to 0.09375
Outputs:
- mixed: bfloat16 [16, 4096], P(None, ('kv', 'tp'))
Inputs may be any that keep to these rules, and one draw needn't show every extreme that they name: `cached_gates`: below a sequence's length, the sum of the log forget gates of the later live cached positions of that sequence and head; zero at and beyond the length. `lengths`: in every draw one sequence has length 16384.
All inputs are finite; a program needn't handle non-finite values.
Results may differ from a plain program's by a relative error of at most 0.015.
Values may be sent and summed in bfloat16 or wider, within the bound.
No kernel may reach another device: no remote copies, remote signals or barrier semaphores. Data moves between devices by JAX's collectives and lax.ppermute only.
A program may use at most 64 MiB of HBM per device.

v0:
```python
import functools

import jax
import jax.numpy as jnp
from jax import lax
from jax.sharding import Mesh
from jax.sharding import PartitionSpec as P

HD = 64
KV = ("kv_0", "kv_1")
KV_TP = ("kv_0", "kv_1", "tp")


EPSILON = 1e-06
NEG_FILL = -1e30


def laid_out(tiles, dim):
    dims = list(tiles.shape[1:])
    dims[dim] *= tiles.shape[0]
    return jnp.moveaxis(tiles, 0, dim).reshape(dims)


def copy_for_each(array, axis):
    copies = jnp.broadcast_to(array, (lax.axis_size(axis), *array.shape))
    return lax.all_to_all(copies, axis, split_axis=0, concat_axis=0, tiled=True)


def collect(array, axis, dim):
    return laid_out(copy_for_each(array, axis), dim)


def over_axes(array, axes):
    return functools.reduce(lax.psum, axes, array)


def collected_together(array, axis):
    leaves = jax.tree.leaves(array)
    order = sorted(range(len(leaves)), key=lambda k: -leaves[k].size)
    width = (1, *leaves[order[0]].shape)[-1]
    lines = [
        jnp.pad(leaves[k].reshape(-1), (0, -leaves[k].size % width)).reshape(-1, width)
        for k in order
    ]
    both, at, found = (copy_for_each(jnp.concatenate(lines), axis), 0, {})
    for k, line in zip(order, lines):
        slab = both[:, at : at + len(line)].reshape(len(both), -1)
        found[k] = slab[:, : leaves[k].size].reshape(-1, *leaves[k].shape)
        at += len(line)
    numbers = iter(range(len(leaves)))
    return jax.tree.map(lambda _: found[next(numbers)], array)


def folded_in_pairs(pieces, combine):
    while len(jax.tree.leaves(pieces)[0]) > 1:
        pieces = jax.vmap(combine)(
            *(jax.tree.map(lambda part: part[side::2], pieces) for side in (0, 1))
        )
    return jax.tree.map(lambda part: part[0], pieces)


def combined_all(array, axis, combine):
    pieces = collected_together(array, axis)
    return folded_in_pairs(pieces, combine)


def in_blocks(array, dim, devices):
    dims = array.shape
    tiles = array.reshape(*dims[:dim], devices, dims[dim] // devices, *dims[dim + 1 :])
    return jnp.moveaxis(tiles, dim, 0)


def summed_on_arrival(array, axis, dim):
    devices = lax.axis_size(axis)
    tiles = lax.all_to_all(in_blocks(array, dim, devices), axis, 0, 0, tiled=True)
    return jnp.sum(tiles, axis=0)


def taken_together(array, axis):
    return copy_for_each(array, axis).astype(jnp.float32).sum(axis=0)


def contract(left_rows, weight_rows):
    return lax.dot_general(
        left_rows, weight_rows, (((1,), (1,)), ((), ())), preferred_element_type=jnp.float32
    )


def join_parts(first, second):
    first_top, first_total, first_sum = first
    second_top, second_total, second_sum = second
    highest = jnp.maximum(first_top, second_top)
    first_factor = jnp.exp(first_top - highest)
    second_factor = jnp.exp(second_top - highest)
    return (
        highest,
        first_factor * first_total + second_factor * second_total,
        first_factor[..., None] * first_sum + second_factor[..., None] * second_sum,
    )


def local(
    tokens,
    attention_gain,
    query_weight,
    key_weight,
    value_weight,
    forget_weight,
    cached_pairs,
    cached_gates,
    lengths,
    output_weight,
    mixer_gain,
    up_weight,
    down_weight,
):
    position_index = lax.axis_index(KV)
    head_index = lax.axis_index("tp")
    sequences, own_columns = tokens.shape
    local_heads = query_weight.shape[0] // HD
    block_columns = query_weight.shape[1]
    model_width = block_columns * lax.axis_size(KV)
    position_count = cached_pairs.shape[-1]
    gain_values = attention_gain.astype(jnp.float32)
    forget_rows = lax.dynamic_slice_in_dim(forget_weight, head_index * local_heads, local_heads, 0)
    block_rows = collect(tokens, "tp", 1)
    block_float = block_rows.astype(jnp.float32)
    block_gain = lax.dynamic_slice_in_dim(
        gain_values, position_index * block_columns, block_columns, 0
    )
    own_block = (block_float * block_gain).astype(jnp.bfloat16)
    forget_block = lax.dynamic_slice_in_dim(
        forget_rows, position_index * block_columns, block_columns, 1
    )
    query_part, key_part, value_part, forget_pre, squares = (
        over_axes(contract(own_block, query_weight), KV),
        over_axes(contract(own_block, key_weight), KV),
        over_axes(contract(own_block, value_weight), KV),
        over_axes(contract(own_block, forget_block), KV),
        over_axes(jnp.sum(block_float * block_float, axis=1, keepdims=True), KV),
    )
    scale_rows = lax.rsqrt(squares / model_width + EPSILON)
    query_heads = (query_part * scale_rows).astype(jnp.bfloat16).reshape(sequences, local_heads, HD)
    key_heads = (key_part * scale_rows).astype(jnp.bfloat16).reshape(sequences, local_heads, HD)
    value_heads = (value_part * scale_rows).astype(jnp.bfloat16).reshape(sequences, local_heads, HD)
    forget = jax.nn.log_sigmoid(forget_pre * scale_rows)
    score_scale = HD ** (-0.5)
    positions = position_index * position_count + jnp.arange(position_count)
    live_mask = positions[None, None, :] < lengths[:, None, None]
    raw_scores = (
        jnp.einsum(
            "shd,shdp->shp", query_heads, cached_pairs[:, :, 0], preferred_element_type=jnp.float32
        )
        * score_scale
    )
    scores = jnp.where(live_mask, raw_scores + cached_gates + forget[:, :, None], NEG_FILL)
    block_top = jnp.max(scores, axis=2)
    weights = jnp.where(live_mask, jnp.exp(scores - block_top[..., None]), 0.0)
    block_total = jnp.sum(weights, axis=2)
    block_sum = jnp.einsum(
        "shp,shdp->shd",
        weights.astype(jnp.bfloat16),
        cached_pairs[:, :, 1],
        preferred_element_type=jnp.float32,
    )
    cache_top, cache_total, summed = combined_all(
        (block_top, block_total, block_sum), KV, join_parts
    )
    own_score = (
        jnp.sum(query_heads.astype(jnp.float32) * key_heads.astype(jnp.float32), axis=2)
        * score_scale
    )
    highest = jnp.maximum(cache_top, own_score)
    cache_factor = jnp.exp(cache_top - highest)
    own_factor = jnp.exp(own_score - highest)
    numerator = cache_factor[..., None] * summed + own_factor[..., None] * value_heads.astype(
        jnp.float32
    )
    denominator = cache_factor * cache_total + own_factor
    attended = (
        (numerator / denominator[..., None])
        .astype(jnp.bfloat16)
        .reshape(sequences, local_heads * HD)
    )
    projected_part = jnp.dot(attended, output_weight, preferred_element_type=jnp.float32)
    mixer_values = mixer_gain.astype(jnp.float32)
    head_total = summed_on_arrival(projected_part, "tp", 1)
    middle_own = (tokens.astype(jnp.float32) + head_total).astype(jnp.bfloat16)
    middle_cols = collect(middle_own, "tp", 1)
    cols_float = middle_cols.astype(jnp.float32)
    cols_gain = lax.dynamic_slice_in_dim(
        mixer_values, position_index * block_columns, block_columns, 0
    )
    scaled_cols = (cols_float * cols_gain).astype(jnp.bfloat16)
    hidden_part, middle_squares = (
        taken_together(contract(scaled_cols, up_weight).astype(jnp.bfloat16), KV).astype(
            jnp.float32
        ),
        taken_together(
            jnp.sum(cols_float * cols_float, axis=1, keepdims=True).astype(jnp.bfloat16), KV
        ).astype(jnp.float32),
    )
    middle_scale = lax.rsqrt(middle_squares / model_width + EPSILON)
    activated = jnp.square(jax.nn.relu(hidden_part * middle_scale)).astype(jnp.bfloat16)
    down_term = jnp.dot(activated, down_weight, preferred_element_type=jnp.float32)
    down_part = summed_on_arrival(down_term, "tp", 1)
    return (middle_own.astype(jnp.float32) + down_part).astype(jnp.bfloat16)


def solution(mesh):
    split = Mesh(mesh.devices.reshape(4, 4, mesh.shape["tp"]), ("kv_0", "kv_1", "tp"))
    return jax.shard_map(
        local,
        mesh=split,
        in_specs=(
            P(None, KV_TP),
            P(),
            P("tp", KV),
            P("tp", KV),
            P("tp", KV),
            P(),
            P(None, "tp", None, None, KV),
            P(None, "tp", KV),
            P(),
            P("tp", KV),
            P(),
            P("tp", KV),
            P("tp", KV),
        ),
        out_specs=P(None, KV_TP),
        check_vma=False,
    )
```

profile of v0, /device:TPU:1, one launch (start us, length us, event | category | flops | bytes accessed | tf_op | source)
XLA Modules:
  0.0 168.6 jit_solution(15296724571440414984)
XLA Ops:
  0.0 1.4 broadcast_in_dim.19
  1.4 16.7 %all-to-all-start = ((bf16[32,16,8]{1,2,0:T(8,128)(2,1)}), bf16[32,16,8]{1,2,0:T(8,128)(2,1)S(1)}, u32[]{:S(2)}, u32[]{:S(2)}) async-start(bf16[32,16,8]{1,2,0:T(8,128)(2,1)} %broadcast_in_dim.19), calls=%async_computation | async-start | bytes 131072 | tf_op jit(solution)/shard_map/all_to_all | solution.py:26
  18.1 0.8 dynamic-slice_convert_fusion.1
  19.0 12.1 %all-to-all-done = bf16[32,16,8]{1,2,0:T(8,128)(2,1)S(1)} async-done(((bf16[32,16,8]{1,2,0:T(8,128)(2,1)}), bf16[32,16,8]{1,2,0:T(8,128)(2,1)S(1)}, u32[]{:S(2)}, u32[]{:S(2)}) %all-to-all-start) | async-done | bytes 8224 | tf_op jit(solution)/shard_map/all_to_all | solution.py:26
  31.2 1.0 fusion.57
  32.2 1.0 fusion.55
  33.2 1.0 fusion.59
  34.2 0.9 convolution_bitcast_fusion.2
  35.1 13.6 %all-reduce.3 = (f32[16,64]{1,0:T(8,128)S(1)}, f32[16,1]{0,1:T(1,128)S(1)}, f32[16,1]{0,1:T(1,128)S(1)}, f32[16,64]{1,0:T(8,128)S(1)}, f32[16,64]{1,0:T(8,128)S(1)}) all-reduce(f32[16,64]{1,0:T(8,128)S(1)} %fusion.59, f32[16,1]{0,1:T(1,128)S(1)} %bitcast.134, ...), channel_id=1, replica_groups=mesh['kv_0'=4,'kv_1'=4,'tp'=32] {'kv_0'}, use_global_device_ids=true, to_apply=%region_0.0 | all-reduce | flops 3104 | bytes 24832 | tf_op jit(solution)/shard_map/psum | solution.py:34
  48.7 13.3 %all-reduce.2 = (f32[16,64]{1,0:T(8,128)S(1)}, f32[16,1]{0,1:T(1,128)S(1)}, f32[16,1]{0,1:T(1,128)S(1)}, f32[16,64]{1,0:T(8,128)S(1)}, f32[16,64]{1,0:T(8,128)S(1)}) all-reduce(f32[16,64]{1,0:T(8,128)S(1)} %get-tuple-element.10, f32[16,1]{0,1:T(1,128)S(1)} %get-tuple-element.11, ...), channel_id=1, replica_groups=mesh['kv_0'=4,'kv_1'=4,'tp'=32] {'kv_1'}, use_global_device_ids=true, to_apply=%region_1.0 | all-reduce | flops 3104 | bytes 24832 | tf_op jit(solution)/shard_map/psum | solution.py:34
  62.2 2.0 %fusion.2 = f32[16,1,1024]{2,1,0:T(1,128)S(1)} fusion(bf16[16,1,2,64,1024]{4,3,2,1,0:T(8,128)(2,1)} %param.19, bf16[16,64,1]{1,0,2:T(8,128)(2,1)S(1)} %get-tuple-element.31), kind=kOutput, calls=%fused_computation.2 | convolution fusion | flops 2097152 | bytes 2164736 | tf_op jit(solution)/shard_map/shd,shdp->shp/dot_general | solution.py:151
  64.2 1.2 fusion.64
  65.4 1.0 fusion.61
  66.4 2.3 %fusion = f32[16,1,64]{2,1,0:T(1,128)S(1)} fusion(bf16[16,1,2,64,1024]{4,3,2,1,0:T(8,128)(2,1)} %param.19, f32[16,1,1024]{2,1,0:T(1,128)S(1)} %get-tuple-element.27, f32[16]{0:T(128)S(1)} %get-tuple-element.26, s32[1024]{0:T(1024)S(1)} %iota_add_fusion, s32[16]{0:T(128)} %param.21), kind=kOutput, calls=%fused_computation | convolution fusion | flops 2162688 | bytes 2171456 | tf_op jit(solution)/shard_map/shp,shdp->shd/dot_general | solution.py:160
  68.8 0.8 reshape.258
  69.5 3.7 %all-to-all-start.1 = ((f32[16,1,1152]{2,1,0:T(1,128)}), f32[16,1,1152]{2,1,0:T(1,128)S(1)}, u32[]{:S(2)}, u32[]{:S(2)}) async-start(f32[16,1,1152]{2,1,0:T(1,128)} %reshape.258), calls=%async_computation.1 | async-start | bytes 147456 | tf_op jit(solution)/shard_map/all_to_all | solution.py:26
  73.4 6.4 %all-to-all-done.1 = f32[16,1,1152]{2,1,0:T(1,128)S(1)} async-done(((f32[16,1,1152]{2,1,0:T(1,128)}), f32[16,1,1152]{2,1,0:T(1,128)S(1)}, u32[]{:S(2)}, u32[]{:S(2)}) %all-to-all-start.1) | async-done | bytes 73760 | tf_op jit(solution)/shard_map/all_to_all | solution.py:26
  80.3 0.8 reduce.9
  82.4 24.9 %all_to_all.35 = f32[32,1,128]{2,1,0:T(1,128)S(1)} all-to-all(f32[32,1,128]{2,1,0:T(1,128)S(1)} %reshape.260), channel_id=1, replica_groups=mesh['kv_0'=4,'kv_1'=4,'tp'=32] {'tp'}, dimensions={0} | all-to-all | bytes 32768 | tf_op jit(solution)/shard_map/all_to_all | solution.py:75
  107.2 0.7 reduce.10
  108.1 0.6 broadcast_in_dim.24
  108.7 4.4 %all-to-all-start.3 = ((bf16[32,16,8]{1,2,0:T(8,128)(2,1)}), bf16[32,16,8]{1,2,0:T(8,128)(2,1)S(1)}, u32[]{:S(2)}, u32[]{:S(2)}) async-start(bf16[32,16,8]{1,2,0:T(8,128)(2,1)} %broadcast_in_dim.24), calls=%async_computation.3 | async-start | bytes 131072 | tf_op jit(solution)/shard_map/all_to_all | solution.py:26
  113.1 0.8 dynamic-slice_convert_fusion
  113.9 12.3 %all-to-all-done.3 = bf16[32,16,8]{1,2,0:T(8,128)(2,1)S(1)} async-done(((bf16[32,16,8]{1,2,0:T(8,128)(2,1)}), bf16[32,16,8]{1,2,0:T(8,128)(2,1)S(1)}, u32[]{:S(2)}, u32[]{:S(2)}) %all-to-all-start.3) | async-done | bytes 8224 | tf_op jit(solution)/shard_map/all_to_all | solution.py:26
  126.2 0.6 broadcast_in_dim.50
  126.8 3.5 %all-to-all-start.5 = ((bf16[16,16,1]{1,2,0:T(2,128)(2,1)}), bf16[16,16,1]{1,2,0:T(2,128)(2,1)S(1)}, u32[]{:S(2)}, u32[]{:S(2)}) async-start(bf16[16,16,1]{1,2,0:T(2,128)(2,1)} %broadcast_in_dim.50), calls=%async_computation.5 | async-start | bytes 16384 | tf_op jit(solution)/shard_map/all_to_all | solution.py:26
  130.6 6.1 %all-to-all-done.5 = bf16[16,16,1]{1,2,0:T(2,128)(2,1)S(1)} async-done(((bf16[16,16,1]{1,2,0:T(2,128)(2,1)}), bf16[16,16,1]{1,2,0:T(2,128)(2,1)S(1)}, u32[]{:S(2)}, u32[]{:S(2)}) %all-to-all-start.5) | async-done | bytes 544 | tf_op jit(solution)/shard_map/all_to_all | solution.py:26
  136.7 0.7 broadcast_in_dim.25
  137.4 3.5 %all-to-all-start.4 = ((bf16[16,16,512]{2,1,0:T(8,128)(2,1)}), bf16[16,16,512]{2,1,0:T(8,128)(2,1)S(1)}, u32[]{:S(2)}, u32[]{:S(2)}) async-start(bf16[16,16,512]{2,1,0:T(8,128)(2,1)} %broadcast_in_dim.25), calls=%async_computation.4 | async-start | bytes 524288 | tf_op jit(solution)/shard_map/all_to_all | solution.py:26
  141.0 7.5 %all-to-all-done.4 = bf16[16,16,512]{2,1,0:T(8,128)(2,1)S(1)} async-done(((bf16[16,16,512]{2,1,0:T(8,128)(2,1)}), bf16[16,16,512]{2,1,0:T(8,128)(2,1)S(1)}, u32[]{:S(2)}, u32[]{:S(2)}) %all-to-all-start.4) | async-done | bytes 262176 | tf_op jit(solution)/shard_map/all_to_all | solution.py:26
  149.0 18.2 %all_to_all.36 = f32[32,1,128]{2,1,0:T(1,128)S(1)} all-to-all(f32[32,1,128]{2,1,0:T(1,128)S(1)} %reshape.262), channel_id=1, replica_groups=mesh['kv_0'=4,'kv_1'=4,'tp'=32] {'tp'}, dimensions={0} | all-to-all | bytes 32768 | tf_op jit(solution)/shard_map/all_to_all | solution.py:75
  167.2 0.7 reduce.11
  (64 shorter events, 3.8 us)
Async XLA Ops:
  0.0 130.3 %copy-start = (bf16[512,256]{1,0:T(8,128)(2,1)S(1)}, bf16[512,256]{1,0:T(8,128)(2,1)}, u32[]{:S(2)}) copy-start(bf16[512,256]{1,0:T(8,128)(2,1)} %param.24) | copy-start | bytes 786436
  0.0 73.2 %copy-start.2 = (bf16[64,256]{1,0:T(8,128)(2,1)S(1)}, bf16[64,256]{1,0:T(8,128)(2,1)}, u32[]{:S(2)}) copy-start(bf16[64,256]{1,0:T(8,128)(2,1)} %param.22) | copy-start | bytes 98308
  1.4 29.8 %all-to-all-start = ((bf16[32,16,8]{1,2,0:T(8,128)(2,1)}), bf16[32,16,8]{1,2,0:T(8,128)(2,1)S(1)}, u32[]{:S(2)}, u32[]{:S(2)}) async-start(bf16[32,16,8]{1,2,0:T(8,128)(2,1)} %broadcast_in_dim.19), calls=%async_computation | async-start | bytes 131072 | tf_op jit(solution)/shard_map/all_to_all | solution.py:26
  62.2 45.9 %copy-start.3 = (bf16[16,8]{0,1:T(8,128)(2,1)S(1)}, bf16[16,8]{0,1:T(8,128)(2,1)}, u32[]{:S(2)}) copy-start(bf16[16,8]{0,1:T(8,128)(2,1)} %param.13) | copy-start | bytes 772
  64.2 84.4 %copy-start.1 = (bf16[512,256]{1,0:T(8,128)(2,1)S(1)}, bf16[512,256]{1,0:T(8,128)(2,1)}, u32[]{:S(2)}) copy-start(bf16[512,256]{1,0:T(8,128)(2,1)} %param.25) | copy-start | bytes 786436
  69.5 10.3 %all-to-all-start.1 = ((f32[16,1,1152]{2,1,0:T(1,128)}), f32[16,1,1152]{2,1,0:T(1,128)S(1)}, u32[]{:S(2)}, u32[]{:S(2)}) async-start(f32[16,1,1152]{2,1,0:T(1,128)} %reshape.258), calls=%async_computation.1 | async-start | bytes 147456 | tf_op jit(solution)/shard_map/all_to_all | solution.py:26
  108.7 17.4 %all-to-all-start.3 = ((bf16[32,16,8]{1,2,0:T(8,128)(2,1)}), bf16[32,16,8]{1,2,0:T(8,128)(2,1)S(1)}, u32[]{:S(2)}, u32[]{:S(2)}) async-start(bf16[32,16,8]{1,2,0:T(8,128)(2,1)} %broadcast_in_dim.24), calls=%async_computation.3 | async-start | bytes 131072 | tf_op jit(solution)/shard_map/all_to_all | solution.py:26
  126.8 9.9 %all-to-all-start.5 = ((bf16[16,16,1]{1,2,0:T(2,128)(2,1)}), bf16[16,16,1]{1,2,0:T(2,128)(2,1)S(1)}, u32[]{:S(2)}, u32[]{:S(2)}) async-start(bf16[16,16,1]{1,2,0:T(2,128)(2,1)} %broadcast_in_dim.50), calls=%async_computation.5 | async-start | bytes 16384 | tf_op jit(solution)/shard_map/all_to_all | solution.py:26
  137.4 11.1 %all-to-all-start.4 = ((bf16[16,16,512]{2,1,0:T(8,128)(2,1)}), bf16[16,16,512]{2,1,0:T(8,128)(2,1)S(1)}, u32[]{:S(2)}, u32[]{:S(2)}) async-start(bf16[16,16,512]{2,1,0:T(8,128)(2,1)} %broadcast_in_dim.25), calls=%async_computation.4 | async-start | bytes 524288 | tf_op jit(solution)/shard_map/all_to_all | solution.py:26
where the time goes:
time: 170 us; the launch traced here: 169 us
  blocking collectives  70 us (41%)
  waiting for transfers between devices  44.5 us (26%)
  starting transfers between devices  31.9 us (19%)
  matrix products  8.99 us (5%)
  other arithmetic  7.33 us (4%)
  local copies, waits for them, and re-layouts  5.71 us (3%)
    all_to_all x5, waiting for transfers between devices, copy_for_each(): return lax.all_to_all(copies, axis, split_axis=0, concat_axis=0, tiled=True)  44.5 us
    all_to_all x2, blocking collectives, summed_on_arrival(): lax.all_to_all(in_blocks(array, dim, devices), axis, 0, 0, tiled=True)  43.1 us
    all_to_all x5, starting transfers between devices, copy_for_each(): return lax.all_to_all(copies, axis, split_axis=0, concat_axis=0, tiled=True)  31.9 us
    psum x2, blocking collectives, over_axes(): return functools.reduce(lax.psum, axes, array)  26.9 us
    dot_general x5, matrix products, contract(): lax.dot_general(left_rows, weight_rows, (((1,), (1,)), ((), ())), preferr...  4.19 us
  transfers between devices with their start and end apart: 5, of which 5 were waited for; matrix products, arithmetic and copies ran while one was open for 1% of the time, Pallas kernels for 0%

commit v1 on v0

v1 whole, which is shorter than its diff:
```python
import jax
import jax.numpy as jnp
from jax import lax
from jax.sharding import Mesh
from jax.sharding import PartitionSpec as P

HD = 64
KV = ("kv_0", "kv_1")
TP = ("z", "core")
KV_TP = (*KV, *TP)

EPSILON = 1e-06
NEG_FILL = -1e30


def copy_for_each(array, axes):
    copies = jnp.broadcast_to(array, (lax.axis_size(axes), *array.shape))
    return lax.all_to_all(copies, axes, split_axis=0, concat_axis=0, tiled=True)


def contract(left_rows, weight_rows):
    return lax.dot_general(
        left_rows, weight_rows, (((1,), (1,)), ((), ())), preferred_element_type=jnp.float32
    )


def lanes(parts, width):
    joined = jnp.concatenate(parts, axis=1)
    return jnp.pad(joined, ((0, 0), (0, width - joined.shape[1])))


def local(
    tokens,
    attention_gain,
    query_weight,
    key_weight,
    value_weight,
    forget_weight,
    cached_pairs,
    cached_gates,
    lengths,
    output_weight,
    mixer_gain,
    up_weight,
    down_weight,
):
    position_index = lax.axis_index(KV)
    head_index = lax.axis_index(TP)
    sequences, own_columns = tokens.shape
    block_columns = query_weight.shape[1]
    model_width = block_columns * lax.axis_size(KV)
    position_count = cached_pairs.shape[-1]

    gathered = copy_for_each(tokens, TP)
    block_float = jnp.moveaxis(gathered, 0, 1).reshape(sequences, -1).astype(jnp.float32)
    start = position_index * block_columns
    block_gain = lax.dynamic_slice_in_dim(attention_gain, start, block_columns, 0)
    own_block = (block_float * block_gain.astype(jnp.float32)).astype(jnp.bfloat16)
    forget_row = lax.dynamic_slice(forget_weight, (head_index, start), (1, block_columns))
    query_part = contract(own_block, query_weight)
    key_part = contract(own_block, key_weight)
    value_part = contract(own_block, value_weight)
    forget_part = contract(own_block, forget_row)
    squares_part = jnp.sum(block_float * block_float, axis=1, keepdims=True)

    first = copy_for_each(lanes([query_part, forget_part, squares_part], 128), KV)
    first = jnp.sum(first, axis=0)
    scale_rows = lax.rsqrt(first[:, HD + 1 : HD + 2] / model_width + EPSILON)
    query = (first[:, :HD] * scale_rows).astype(jnp.bfloat16)
    forget = jax.nn.log_sigmoid(first[:, HD : HD + 1] * scale_rows)
    score_scale = HD ** (-0.5)
    own_part = jnp.sum(query.astype(jnp.float32) * key_part, axis=1, keepdims=True)

    positions = position_index * position_count + jnp.arange(position_count)
    live_mask = positions[None, :] < lengths[:, None]
    raw_scores = jnp.einsum(
        "sd,sdp->sp", query, cached_pairs[:, 0, 0], preferred_element_type=jnp.float32
    )
    scores = jnp.where(live_mask, raw_scores * score_scale + cached_gates[:, 0], NEG_FILL)
    block_top = jnp.max(scores, axis=1, keepdims=True)
    weights = jnp.where(live_mask, jnp.exp(scores - block_top), 0.0)
    block_total = jnp.sum(weights, axis=1, keepdims=True)
    block_sum = jnp.einsum(
        "sp,sdp->sd",
        weights.astype(jnp.bfloat16),
        cached_pairs[:, 0, 1],
        preferred_element_type=jnp.float32,
    )

    second = copy_for_each(
        lanes([block_sum, value_part, block_top, block_total, own_part], 256), KV
    )
    tops = second[:, :, 2 * HD] + forget[:, 0][None]
    own_score = jnp.sum(second[:, :, 2 * HD + 2], axis=0) * scale_rows[:, 0] * score_scale
    value_new = jnp.sum(second[:, :, HD : 2 * HD], axis=0) * scale_rows
    value_new = value_new.astype(jnp.bfloat16).astype(jnp.float32)
    highest = jnp.maximum(jnp.max(tops, axis=0), own_score)
    factors = jnp.exp(tops - highest[None])
    own_factor = jnp.exp(own_score - highest)
    numerator = jnp.sum(factors[..., None] * second[:, :, :HD], axis=0)
    numerator = numerator + own_factor[:, None] * value_new
    denominator = jnp.sum(factors * second[:, :, 2 * HD + 1], axis=0) + own_factor
    attended = (numerator / denominator[:, None]).astype(jnp.bfloat16)

    projected = jnp.dot(attended, output_weight, preferred_element_type=jnp.float32)
    projected = jnp.sum(copy_for_each(projected, "core"), axis=0).astype(jnp.bfloat16)
    projected = jnp.sum(copy_for_each(projected, "z").astype(jnp.float32), axis=0)
    middle = (block_float + projected).astype(jnp.bfloat16)
    middle_float = middle.astype(jnp.float32)
    middle_gain = lax.dynamic_slice_in_dim(mixer_gain, start, block_columns, 0)
    scaled_middle = (middle_float * middle_gain.astype(jnp.float32)).astype(jnp.bfloat16)

    hidden_part = contract(scaled_middle, up_weight)
    hidden_units = hidden_part.shape[1]
    middle_squares = jnp.sum(middle_float * middle_float, axis=1, keepdims=True)
    third = lanes([hidden_part, middle_squares], hidden_units + 128).astype(jnp.bfloat16)
    third = jnp.sum(copy_for_each(third, KV).astype(jnp.float32), axis=0)
    middle_scale = lax.rsqrt(third[:, hidden_units : hidden_units + 1] / model_width + EPSILON)
    activated = jnp.square(jax.nn.relu(third[:, :hidden_units] * middle_scale)).astype(jnp.bfloat16)

    down_term = jnp.dot(activated, down_weight, preferred_element_type=jnp.float32)
    tiles = jnp.moveaxis(down_term.reshape(sequences, -1, own_columns), 1, 0)
    tiles = lax.all_to_all(tiles, TP, 0, 0, tiled=True)
    middle_own = lax.dynamic_slice_in_dim(middle_float, head_index * own_columns, own_columns, 1)
    return (middle_own + jnp.sum(tiles, axis=0)).astype(jnp.bfloat16)


def solution(mesh):
    split = Mesh(mesh.devices.reshape(4, 4, 16, 2), KV_TP)
    return jax.shard_map(
        local,
        mesh=split,
        in_specs=(
            P(None, KV_TP),
            P(),
            P(TP, KV),
            P(TP, KV),
            P(TP, KV),
            P(),
            P(None, TP, None, None, KV),
            P(None, TP, KV),
            P(),
            P(TP, KV),
            P(),
            P(TP, KV),
            P(TP, KV),
        ),
        out_specs=P(None, KV_TP),
        check_vma=False,
    )
```

time: 170 us -> 126 us (0.74)
  blocking collectives: 70 us -> 43.5 us
  waiting for transfers between devices: 44.5 us -> 29.7 us
  other arithmetic: 7.33 us -> 5.37 us
    psum x2 -> x0, blocking collectives: 26.9 us -> none  [over_axes(): return functools.reduce(lax.psum, axes, array)]
    all_to_all x5 -> x3, waiting for transfers between devices: 44.5 us -> 29.7 us  [the longest x2 18 us: copy_for_each(): return lax.all_to_all(copies, axes, split_axis=0, concat_axis=0, tiled=True)]
    all_to_all x5 -> x3, starting transfers between devices: 31.9 us -> 32.5 us  [the longest x2 23.5 us: copy_for_each(): return lax.all_to_all(copies, axes, split_axis=0, concat_axis=0, tiled=True)]
    all_to_all x2 -> x4, blocking collectives: 43.1 us -> 43.5 us  [copy_for_each(): return lax.all_to_all(copies, axes, split_axis=0, concat_axis=0, tiled=True)]
  transfers between devices with their start and end apart: 5 -> 3, of which waited for: 5 -> 3; matrix products, arithmetic and copies ran while one was open for 1% -> 1% of each run, Pallas kernels for 0% -> 0%
where the time goes in v1:
time: 126 us; the launch traced here: 125 us
  blocking collectives  43.5 us (35%)
  starting transfers between devices  32.5 us (26%)
  waiting for transfers between devices  29.7 us (24%)
  matrix products  9.04 us (7%)
  other arithmetic  5.37 us (4%)
  local copies, waits for them, and re-layouts  4.69 us (4%)
    all_to_all x4, blocking collectives, copy_for_each(): return lax.all_to_all(copies, axes, split_axis=0, concat_axis=0, tiled=True)  43.5 us
    all_to_all x2, starting transfers between devices, copy_for_each(): return lax.all_to_all(copies, axes, split_axis=0, concat_axis=0, tiled=True)  23.5 us
    all_to_all x2, waiting for transfers between devices, copy_for_each(): return lax.all_to_all(copies, axes, split_axis=0, concat_axis=0, tiled=True)  18 us
    all_to_all x1, waiting for transfers between devices, local(): tiles = lax.all_to_all(tiles, TP, 0, 0, tiled=True)  11.8 us
    all_to_all x1, starting transfers between devices, local(): tiles = lax.all_to_all(tiles, TP, 0, 0, tiled=True)  9.05 us
    dot_general x5, matrix products, contract(): lax.dot_general(left_rows, weight_rows, (((1,), (1,)), ((), ())), preferr...  4.34 us
  transfers between devices with their start and end apart: 3, of which 3 were waited for; matrix products, arithmetic and copies ran while one was open for 1% of the time, Pallas kernels for 0%

profile of v1, /device:TPU:1, one launch (start us, length us, event | category | flops | bytes accessed | tf_op | source)
XLA Modules:
  0.0 125.1 jit_solution(12706072452868425001)
XLA Ops:
  0.0 1.4 %broadcast_in_dim.49 = bf16[32,16,8]{1,2,0:T(8,128)(2,1)} broadcast(bf16[16,8]{0,1:T(8,128)(2,1)} %param.13), dimensions={1,2} | broadcast | bytes 8448 | tf_op jit(solution)/shard_map/broadcast_in_dim | solution.py:17
  1.4 16.7 %all-to-all-start = ((bf16[32,16,8]{1,2,0:T(8,128)(2,1)}), bf16[32,16,8]{1,2,0:T(8,128)(2,1)S(1)}, u32[]{:S(2)}, u32[]{:S(2)}) async-start(bf16[32,16,8]{1,2,0:T(8,128)(2,1)} %broadcast_in_dim.49), calls=%async_computation | async-start | bytes 131072 | tf_op jit(solution)/shard_map/all_to_all | solution.py:18
  18.1 0.8 dynamic-slice_convert_fusion
  19.0 12.1 %all-to-all-done = bf16[32,16,8]{1,2,0:T(8,128)(2,1)S(1)} async-done(((bf16[32,16,8]{1,2,0:T(8,128)(2,1)}), bf16[32,16,8]{1,2,0:T(8,128)(2,1)S(1)}, u32[]{:S(2)}, u32[]{:S(2)}) %all-to-all-start) | async-done | bytes 8224 | tf_op jit(solution)/shard_map/all_to_all | solution.py:18
  31.2 1.0 fusion.62
  32.3 0.9 convolution_bitcast_fusion.1
  33.3 0.7 broadcast_in_dim.51
  33.9 6.8 %all-to-all-start.1 = ((f32[16,16,128]{2,1,0:T(8,128)}), f32[16,16,128]{2,1,0:T(8,128)S(1)}, u32[]{:S(2)}, u32[]{:S(2)}) async-start(f32[16,16,128]{2,1,0:T(8,128)} %broadcast_in_dim.51), calls=%async_computation.1 | async-start | bytes 262144 | tf_op jit(solution)/shard_map/all_to_all | solution.py:18
  40.7 1.0 fusion.60
  41.7 5.8 %all-to-all-done.1 = f32[16,16,128]{2,1,0:T(8,128)S(1)} async-done(((f32[16,16,128]{2,1,0:T(8,128)}), f32[16,16,128]{2,1,0:T(8,128)S(1)}, u32[]{:S(2)}, u32[]{:S(2)}) %all-to-all-start.1) | async-done | bytes 131104 | tf_op jit(solution)/shard_map/all_to_all | solution.py:18
  47.6 0.2 fusion.38
  47.9 1.1 fusion.6
  49.1 2.0 %fusion.2 = f32[16,1,1024]{2,1,0:T(1,128)S(1)} fusion(bf16[16,1,2,64,1024]{4,3,2,1,0:T(8,128)(2,1)} %param.19, bf16[16,64,1]{1,0,2:T(8,128)(2,1)S(1)} %fusion.57), kind=kOutput, calls=%fused_computation.2 | convolution fusion | flops 2097152 | bytes 2164736 | tf_op jit(solution)/shard_map/sd,sdp->sp/dot_general | solution.py:76
  51.1 1.1 fusion.64
  52.1 0.9 fusion.24
  53.0 2.2 %fusion = f32[16,1,64]{2,1,0:T(1,128)S(1)} fusion(bf16[16,1,2,64,1024]{4,3,2,1,0:T(8,128)(2,1)} %param.19, bf16[16,1024,1]{1,0,2:T(8,128)(2,1)S(1)} %get-tuple-element.17), kind=kOutput, calls=%fused_computation | convolution fusion | flops 2097152 | bytes 2134016 | tf_op jit(solution)/shard_map/sp,sdp->sd/dot_general | solution.py:83
  55.5 10.6 %all_to_all.35 = f32[16,16,256]{2,1,0:T(8,128)S(1)} all-to-all(f32[16,16,256]{2,1,0:T(8,128)S(1)} %broadcast_in_dim.57), channel_id=1, replica_groups=mesh['kv_0'=4,'kv_1'=4,'z'=16,'core'=2] {'kv_0','kv_1'}, dimensions={0} | all-to-all | bytes 524288 | tf_op jit(solution)/shard_map/all_to_all | solution.py:18
  66.2 0.2 fusion.65
  66.5 0.2 copy.135
  67.1 0.2 fusion.58
  67.4 0.2 fusion.50
  67.6 7.5 %all_to_all.36 = f32[2,16,256]{2,1,0:T(8,128)S(1)} all-to-all(f32[2,16,256]{2,1,0:T(8,128)S(1)} %broadcast_in_dim.58), channel_id=1, replica_groups=mesh['kv_0'=4,'kv_1'=4,'z'=16,'core'=2] {'core'}, dimensions={0} | all-to-all | bytes 65536 | tf_op jit(solution)/shard_map/all_to_all | solution.py:18
  75.2 14.8 %all_to_all.37 = bf16[16,16,256]{2,1,0:T(8,128)(2,1)S(1)} all-to-all(bf16[16,16,256]{2,1,0:T(8,128)(2,1)S(1)} %broadcast_in_dim.59), channel_id=1, replica_groups=mesh['kv_0'=4,'kv_1'=4,'z'=16,'core'=2] {'z'}, dimensions={0} | all-to-all | bytes 262144 | tf_op jit(solution)/shard_map/all_to_all | solution.py:18
  90.3 0.3 convolution_convert_fusion
  90.6 10.5 %all_to_all.38 = bf16[16,16,640]{2,1,0:T(8,128)(2,1)S(1)} all-to-all(bf16[16,16,640]{2,1,0:T(8,128)(2,1)S(1)} %broadcast_in_dim.61), channel_id=1, replica_groups=mesh['kv_0'=4,'kv_1'=4,'z'=16,'core'=2] {'kv_0','kv_1'}, dimensions={0} | all-to-all | bytes 655360 | tf_op jit(solution)/shard_map/all_to_all | solution.py:18
  101.3 0.3 fusion.66
  101.6 0.7 reshape.69
  102.3 9.0 %all-to-all-start.6 = ((f32[32,1,128]{2,1,0:T(1,128)}), f32[32,1,128]{2,1,0:T(1,128)S(1)}, u32[]{:S(2)}, u32[]{:S(2)}) async-start(f32[32,1,128]{2,1,0:T(1,128)} %reshape.69), calls=%async_computation.6 | async-start | bytes 32768 | tf_op jit(solution)/shard_map/all_to_all | solution.py:123
  111.4 11.8 %all-to-all-done.6 = f32[32,1,128]{2,1,0:T(1,128)S(1)} async-done(((f32[32,1,128]{2,1,0:T(1,128)}), f32[32,1,128]{2,1,0:T(1,128)S(1)}, u32[]{:S(2)}, u32[]{:S(2)}) %all-to-all-start.6) | async-done | bytes 16416 | tf_op jit(solution)/shard_map/all_to_all | solution.py:123
  123.2 0.5 broadcast.91
  123.7 0.7 reduce.13
  124.5 0.6 add_convert_fusion
  (42 shorter events, 2.0 us)
Async XLA Ops:
  0.0 90.3 %copy-start = (bf16[512,256]{1,0:T(8,128)(2,1)S(1)}, bf16[512,256]{1,0:T(8,128)(2,1)}, u32[]{:S(2)}) copy-start(bf16[512,256]{1,0:T(8,128)(2,1)} %param.24) | copy-start | bytes 786436
  1.4 29.8 %all-to-all-start = ((bf16[32,16,8]{1,2,0:T(8,128)(2,1)}), bf16[32,16,8]{1,2,0:T(8,128)(2,1)S(1)}, u32[]{:S(2)}, u32[]{:S(2)}) async-start(bf16[32,16,8]{1,2,0:T(8,128)(2,1)} %broadcast_in_dim.49), calls=%async_computation | async-start | bytes 131072 | tf_op jit(solution)/shard_map/all_to_all | solution.py:18
  32.3 35.2 %copy-start.2 = (bf16[64,256]{1,0:T(8,128)(2,1)S(1)}, bf16[64,256]{1,0:T(8,128)(2,1)}, u32[]{:S(2)}) copy-start(bf16[64,256]{1,0:T(8,128)(2,1)} %param.22) | copy-start | bytes 98308
  33.9 13.6 %all-to-all-start.1 = ((f32[16,16,128]{2,1,0:T(8,128)}), f32[16,16,128]{2,1,0:T(8,128)S(1)}, u32[]{:S(2)}, u32[]{:S(2)}) async-start(f32[16,16,128]{2,1,0:T(8,128)} %broadcast_in_dim.51), calls=%async_computation.1 | async-start | bytes 262144 | tf_op jit(solution)/shard_map/all_to_all | solution.py:18
  51.0 50.3 %copy-start.1 = (bf16[512,256]{1,0:T(8,128)(2,1)S(1)}, bf16[512,256]{1,0:T(8,128)(2,1)}, u32[]{:S(2)}) copy-start(bf16[512,256]{1,0:T(8,128)(2,1)} %param.25) | copy-start | bytes 786436
  102.3 20.8 %all-to-all-start.6 = ((f32[32,1,128]{2,1,0:T(1,128)}), f32[32,1,128]{2,1,0:T(1,128)S(1)}, u32[]{:S(2)}, u32[]{:S(2)}) async-start(f32[32,1,128]{2,1,0:T(1,128)} %reshape.69), calls=%async_computation.6 | async-start | bytes 32768 | tf_op jit(solution)/shard_map/all_to_all | solution.py:123

commit v2 on v1

v2 whole, which is shorter than its diff:
```python
import functools

import jax
import jax.numpy as jnp
from jax import lax
from jax.experimental import pallas as pl
from jax.experimental.pallas import tpu as pltpu
from jax.sharding import Mesh
from jax.sharding import PartitionSpec as P

HD = 64
KV = ("kv_0", "kv_1")
TP = ("z", "core")
KV_TP = (*KV, *TP)
LANES = 128

COST = 1 << 34
EPSILON = 1e-06
NEG_FILL = -1e30
F32 = jnp.float32
BF16 = jnp.bfloat16


def exchange(copies, axes):
    return lax.all_to_all(copies, axes, split_axis=0, concat_axis=0, tiled=True)


def near(array):
    return pltpu.with_memory_space_constraint(array, pltpu.VMEM)


def call(body, outs, name, scratch=()):
    return pl.pallas_call(
        body,
        out_shape=[jax.ShapeDtypeStruct(shape, dtype) for shape, dtype in outs],
        scratch_shapes=list(scratch),
        name=name,
        cost_estimate=pl.CostEstimate(flops=COST, bytes_accessed=COST // 256, transcendentals=0),
        compiler_params=pltpu.CompilerParams(vmem_limit_bytes=24 << 20),
    )


def rows_dot(left, right):
    return lax.dot_general(left, right, (((1,), (1,)), ((), ())), preferred_element_type=F32)


def iota(shape, dim):
    return lax.broadcasted_iota(jnp.int32, shape, dim)


def block_gain(gain_ref, block):
    gains = gain_ref[...].astype(F32)
    rows = iota(gains.shape, 0)
    first = jnp.sum(jnp.where(rows == 2 * block, gains, 0.0), axis=0, keepdims=True)
    second = jnp.sum(jnp.where(rows == 2 * block + 1, gains, 0.0), axis=0, keepdims=True)
    return jnp.concatenate([first, second], axis=1)


def spread_body(tokens, out):
    rows = tokens[...].astype(F32)
    line = jnp.concatenate([rows[at : at + 1] for at in range(rows.shape[0])], axis=1)
    out[...] = jnp.broadcast_to(line[None], out.shape)


def project_body(got, gain, query_w, key_w, value_w, forget_w, first_out, parts_out, block_out):
    position = lax.axis_index("kv_0") * 4 + lax.axis_index("kv_1")
    head = lax.axis_index("z") * 2 + lax.axis_index("core")
    peers = got.shape[0]
    sequences = block_out.shape[0]
    columns = LANES // sequences
    spread = jnp.broadcast_to(got[...], (peers, columns, LANES)).reshape(peers * columns, LANES)
    keep = (iota(spread.shape, 1) // sequences) == (iota(spread.shape, 0) % columns)
    fold = (iota((sequences, LANES), 1) % sequences) == iota((sequences, LANES), 0)
    block = rows_dot(
        jnp.where(fold, 1.0, 0.0).astype(BF16), jnp.where(keep, spread, 0.0).astype(BF16)
    )
    block_out[...] = block
    own = (block * block_gain(gain, position)).astype(BF16)
    query = rows_dot(own, query_w[...])
    key = rows_dot(own, key_w[...])
    value = rows_dot(own, value_w[...])
    width = block.shape[1]
    gate_rows = forget_w[:, pl.ds(pl.multiple_of(position * width, width), width)]
    gates = rows_dot(own, gate_rows)
    gate = jnp.sum(jnp.where(iota(gates.shape, 1) == head, gates, 0.0), axis=1, keepdims=True)
    squares = jnp.sum(block * block, axis=1, keepdims=True)
    lane = iota((sequences, LANES - HD), 1)
    rest = jnp.where(lane == 0, gate, jnp.where(lane == 1, squares, 0.0))
    line = jnp.concatenate([query, rest], axis=1)
    first_out[...] = jnp.broadcast_to(line[None], first_out.shape)
    parts_out[...] = jnp.concatenate([key, value], axis=1)


def pieces(column):
    high = column.astype(BF16).astype(F32)
    middle = (column - high).astype(BF16).astype(F32)
    return high, middle, column - high - middle


def attend_body(model_width, got, parts, pairs, gates, lengths, second_out, row_out):
    position = lax.axis_index("kv_0") * 4 + lax.axis_index("kv_1")
    sequences = parts.shape[0]
    count = gates.shape[2]
    line = jnp.sum(got[...], axis=0)
    scale = lax.rsqrt(line[:, HD + 1 : HD + 2] / model_width + EPSILON)
    query = (line[:, :HD] * scale).astype(BF16)
    forget = jax.nn.log_sigmoid(line[:, HD : HD + 1] * scale)
    wide = sequences * HD
    own_group = (iota((sequences, wide), 1) // HD) == iota((sequences, wide), 0)
    spread = jnp.concatenate([query.astype(F32)] * sequences, axis=1)
    spread = jnp.where(own_group, spread, 0.0).astype(BF16)
    keys = pairs[:, 0, 0].reshape(wide, count)
    raw = jnp.dot(spread, keys, preferred_element_type=F32)
    diagonal = iota((sequences, sequences), 0) == iota((sequences, sequences), 1)
    ends = jnp.broadcast_to(lengths[...].reshape(1, sequences), (sequences, sequences))
    ends = jnp.sum(jnp.where(diagonal, ends, 0), axis=1, keepdims=True) - position * count
    live = iota((sequences, count), 1) < ends
    scores = jnp.where(live, raw * HD ** (-0.5) + gates[:, 0, :], NEG_FILL)
    top = jnp.max(scores, axis=1, keepdims=True)
    weights = jnp.where(live, jnp.exp(scores - top), 0.0)
    total = jnp.sum(weights, axis=1, keepdims=True)
    values = pairs[:, 0, 1].reshape(wide, count)
    sums = jnp.where(own_group, rows_dot(weights.astype(BF16), values), 0.0)
    folded = sums[:, :LANES]
    for at in range(LANES, wide, LANES):
        folded = folded + sums[:, at : at + LANES]
    block_sum = folded[:, :HD] + folded[:, HD:]
    own = jnp.sum(query.astype(F32) * parts[:, :HD], axis=1, keepdims=True)
    lane = iota((sequences, LANES), 1)
    stats = jnp.zeros((sequences, LANES), F32)
    for at, piece in enumerate((*pieces(top), *pieces(total), *pieces(own))):
        stats = jnp.where(lane == at, piece, stats)
    out = jnp.concatenate([block_sum, parts[:, HD:], stats], axis=1).astype(BF16)
    second_out[...] = jnp.broadcast_to(out[None], second_out.shape)
    row_out[...] = jnp.where(lane == 0, forget, jnp.where(lane == 1, scale, 0.0))


def combine_body(got, row, output_w, out):
    sums = got[:, :, :HD].astype(F32)
    value_parts = got[:, :, HD:LANES].astype(F32)
    stats = got[:, :, LANES:].astype(F32)
    forget, scale = row[:, 0:1], row[:, 1:2]

    def stat(at):
        return stats[:, :, at : at + 1] + stats[:, :, at + 1 : at + 2] + stats[:, :, at + 2 : at + 3]

    tops = stat(0) + forget[None]
    own_score = jnp.sum(stat(6), axis=0) * scale * HD ** (-0.5)
    value_new = (jnp.sum(value_parts, axis=0) * scale).astype(BF16).astype(F32)
    highest = jnp.maximum(jnp.max(tops, axis=0), own_score)
    factors = jnp.exp(tops - highest[None])
    own_factor = jnp.exp(own_score - highest)
    numerator = jnp.sum(factors * sums, axis=0) + own_factor * value_new
    denominator = jnp.sum(factors * stat(3), axis=0) + own_factor
    attended = (numerator / denominator).astype(BF16)
    projected = jnp.dot(attended, output_w[...], preferred_element_type=F32)
    out[...] = jnp.broadcast_to(projected[None], out.shape)


def mix_body(got, block, gain, up_w, third_out, middle_out):
    position = lax.axis_index("kv_0") * 4 + lax.axis_index("kv_1")
    projected = jnp.sum(got[...].astype(F32), axis=0)
    middle = (block[...] + projected).astype(BF16)
    middle_out[...] = middle
    wide = middle.astype(F32)
    scaled = (wide * block_gain(gain, position)).astype(BF16)
    hidden = rows_dot(scaled, up_w[...])
    squares = jnp.sum(wide * wide, axis=1, keepdims=True)
    lane = iota((wide.shape[0], LANES), 1)
    stats = jnp.zeros(lane.shape, F32)
    for at, piece in enumerate(pieces(squares)):
        stats = jnp.where(lane == at, piece, stats)
    out = jnp.concatenate([hidden, stats], axis=1).astype(BF16)
    third_out[...] = jnp.broadcast_to(out[None], third_out.shape)


def down_body(model_width, got, down_w, out, turned):
    summed = jnp.sum(got[...].astype(F32), axis=0)
    units = down_w.shape[0]
    squares = summed[:, units : units + 1] + summed[:, units + 1 : units + 2]
    squares = squares + summed[:, units + 2 : units + 3]
    scale = lax.rsqrt(squares / model_width + EPSILON)
    activated = jnp.square(jax.nn.relu(summed[:, :units] * scale)).astype(BF16)
    sequences = activated.shape[0]
    down = jnp.dot(activated, down_w[...], preferred_element_type=F32)
    turned[...] = down.T
    peers = out.shape[0]
    columns = LANES // sequences
    lines = [turned[pl.ds(at, peers, stride=columns), :] for at in range(columns)]
    out[...] = jnp.concatenate(lines, axis=1).reshape(out.shape)


def finish_body(got, middle, out):
    head = lax.axis_index("z") * 2 + lax.axis_index("core")
    columns, sequences = out.shape
    line = jnp.sum(got[...], axis=0)
    own_shape = (columns, middle.shape[1])
    chosen = iota(own_shape, 1) == iota(own_shape, 0) + head * columns
    own = rows_dot(jnp.where(chosen, 1.0, 0.0).astype(BF16), middle[...])
    down = jnp.concatenate(
        [line[:, at * sequences : (at + 1) * sequences] for at in range(columns)], axis=0
    )
    out[...] = (own + down).astype(BF16)


def local(
    tokens,
    attention_gain,
    query_weight,
    key_weight,
    value_weight,
    forget_weight,
    cached_pairs,
    cached_gates,
    lengths,
    output_weight,
    mixer_gain,
    up_weight,
    down_weight,
):
    sequences, own_columns = tokens.shape
    blocks, heads = lax.axis_size(KV), lax.axis_size(TP)
    width = query_weight.shape[1]
    model_width = width * blocks
    hidden_units = up_weight.shape[0]

    (line,) = call(spread_body, [((heads, 1, sequences * own_columns), F32)], "spread")(tokens.T)
    got = exchange(line, TP)
    first, parts, block = call(
        project_body,
        [((blocks, sequences, LANES), F32), ((sequences, LANES), F32), ((sequences, width), F32)],
        "project",
    )(
        got,
        near(attention_gain.reshape(-1, LANES)),
        near(query_weight),
        near(key_weight),
        near(value_weight),
        near(forget_weight),
    )
    got = exchange(first, KV)
    second, row = call(
        functools.partial(attend_body, model_width),
        [((blocks, sequences, 2 * LANES), BF16), ((sequences, LANES), F32)],
        "attend",
    )(got, parts, near(cached_pairs), near(cached_gates), near(lengths))
    got = exchange(second, KV)
    (projected,) = call(combine_body, [((2, sequences, width), F32)], "combine")(
        got, row, near(output_weight)
    )
    projected = jnp.sum(exchange(projected, "core"), axis=0).astype(BF16)
    got = exchange(jnp.broadcast_to(projected, (lax.axis_size("z"), *projected.shape)), "z")
    third, middle = call(
        mix_body,
        [((blocks, sequences, hidden_units + LANES), BF16), ((sequences, width), BF16)],
        "mix",
    )(got, block, near(mixer_gain.reshape(-1, LANES)), near(up_weight))
    got = exchange(third, KV)
    (down,) = call(
        functools.partial(down_body, model_width),
        [((heads, 1, LANES), F32)],
        "down",
        [pltpu.VMEM((width, sequences), F32)],
    )(got, near(down_weight))
    got = exchange(down, TP)
    (out,) = call(finish_body, [((own_columns, sequences), BF16)], "finish")(got, middle)
    return out.T


def solution(mesh):
    split = Mesh(mesh.devices.reshape(4, 4, 16, 2), KV_TP)
    return jax.shard_map(
        local,
        mesh=split,
        in_specs=(
            P(None, KV_TP),
            P(),
            P(TP, KV),
            P(TP, KV),
            P(TP, KV),
            P(),
            P(None, TP, None, None, KV),
            P(None, TP, KV),
            P(),
            P(TP, KV),
            P(),
            P(TP, KV),
            P(TP, KV),
        ),
        out_specs=P(None, KV_TP),
        check_vma=False,
    )
```

time: 126 us -> 110 us (0.87)
  blocking collectives: 43.5 us -> 105 us
  starting transfers between devices: 32.5 us -> 0 us
  waiting for transfers between devices: 29.7 us -> 0 us
  matrix products: 9.04 us -> 0 us
  other arithmetic: 5.37 us -> 0.01 us
  local copies, waits for them, and re-layouts: 4.69 us -> 0.75 us
  Pallas kernels: 0 us -> 3.64 us
    all_to_all x4 -> x7, blocking collectives: 43.5 us -> 105 us  [exchange(): return lax.all_to_all(copies, axes, split_axis=0, concat_axis=0, tiled=True)]
    all_to_all x3 -> x0, starting transfers between devices: 32.5 us -> none  [the longest x2 23.5 us: copy_for_each(): return lax.all_to_all(copies, axes, split_axis=0, concat_axis=0, tiled=True)]
    all_to_all x3 -> x0, waiting for transfers between devices: 29.7 us -> none  [the longest x2 18 us: copy_for_each(): return lax.all_to_all(copies, axes, split_axis=0, concat_axis=0, tiled=True)]
    dot_general x9 -> x0, matrix products: 9.04 us -> none  [the longest x5 4.34 us: contract(): lax.dot_general(left_rows, weight_rows, (((1,), (1,)), ((), ())), preferr...]
    pallas_call x0 -> x7, Pallas kernels: none -> 3.64 us  [the longest x1 1.21 us: local(): call(functools.partial(attend_body, model_width), [((blocks, sequences, 2...]
    broadcast_in_dim x11 -> x1, local copies, waits for them, and re-layouts: 2.52 us -> 0.01 us  [local(): jnp.broadcast_to(projected, (lax.axis_size('z'), *projected.shape))]
    convert_element_type x4 -> x0, other arithmetic: 1.45 us -> none  [the longest x1 0.78 us: local(): middle_gain.astype(jnp.float32)]
  transfers between devices with their start and end apart: 3 -> 0, of which waited for: 3 -> 0; matrix products, arithmetic and copies ran while one was open for 1% -> 0% of each run, Pallas kernels for 0% -> 0%
where the time goes in v2:
time: 110 us
  blocking collectives  105 us (95%)
  Pallas kernels  3.64 us (3%)
    all_to_all x7, blocking collectives, exchange(): return lax.all_to_all(copies, axes, split_axis=0, concat_axis=0, tiled=True)  105 us

profile of v2, /device:TPU:1, one launch (start us, length us, event | category | flops | bytes accessed | tf_op | source)
XLA Modules:
  0.0 109.7 jit_solution(7184526857682273136)
XLA Ops:
  0.0 0.7 copy-done.11
  0.7 0.0 copy-start.9
  0.7 0.1 spread.1
  0.8 28.5 %all_to_all.35.got = f32[32,1,128]{2,1,0:T(1,128)S(1)} all-to-all(f32[32,1,128]{2,1,0:T(1,128)S(1)} %spread.1), channel_id=1, replica_groups=mesh['kv_0'=4,'kv_1'=4,'z'=16,'core'=2] {'z','core'}, dimensions={0} | all-to-all | bytes 32768 | tf_op jit(solution)/shard_map/all_to_all | solution.py:25
  29.3 0.0 copy-done.1
  29.3 0.0 copy-done.5
  29.3 0.0 copy-done.6
  29.3 0.0 copy-done.7
  29.3 0.0 copy-done.9
  29.3 0.0 copy-start
  29.3 0.0 copy-start.4
  29.3 0.0 copy-start.12
  29.4 0.4 project.1
  29.8 13.7 %all_to_all.36.got = f32[16,16,128]{2,1,0:T(8,128)S(1)} all-to-all(f32[16,16,128]{2,1,0:T(8,128)S(1)} %get-tuple-element.12), channel_id=1, replica_groups=mesh['kv_0'=4,'kv_1'=4,'z'=16,'core'=2] {'kv_0','kv_1'}, dimensions={0} | all-to-all | bytes 262144 | tf_op jit(solution)/shard_map/all_to_all | solution.py:25
  43.5 0.0 copy-done
  43.5 0.0 copy-done.4
  43.5 0.0 copy-done.12
  43.5 0.0 copy-start.8
  43.5 1.2 %attend.1 = (bf16[16,16,256]{2,1,0:T(8,128)(2,1)S(1)}, f32[16,128]{1,0:T(8,128)S(1)}) custom-call(f32[16,16,128]{2,1,0:T(8,128)S(1)} %all_to_all.36.got, f32[16,128]{1,0:T(8,128)S(1)} %get-tuple-element.13.parts, bf16[16,1,2,64,1024]{4,3,2,1,0:T(8,128)(2,1)S(1)} %copy-done, f32[16,1,1024]{2,1,0:T(1,128)S(1)} %copy-done.4, s32[16]{0:T(128)S(1)} %copy-done.12), custom_call_target="tpu_custom_call" | custom-call | flops 17179869184 | bytes 67108864 | tf_op jit(solution)/shard_map/attend/pallas_call | solution.py:242
  44.7 10.0 %all_to_all.37.got = bf16[16,16,256]{2,1,0:T(8,128)(2,1)S(1)} all-to-all(bf16[16,16,256]{2,1,0:T(8,128)(2,1)S(1)} %get-tuple-element.14), channel_id=1, replica_groups=mesh['kv_0'=4,'kv_1'=4,'z'=16,'core'=2] {'kv_0','kv_1'}, dimensions={0} | all-to-all | bytes 262144 | tf_op jit(solution)/shard_map/all_to_all | solution.py:25
  54.7 0.0 copy-done.8
  54.7 0.5 combine.1
  55.2 6.9 %all_to_all.38 = f32[2,16,256]{2,1,0:T(8,128)S(1)} all-to-all(f32[2,16,256]{2,1,0:T(8,128)S(1)} %combine.1), channel_id=1, replica_groups=mesh['kv_0'=4,'kv_1'=4,'z'=16,'core'=2] {'core'}, dimensions={0} | all-to-all | bytes 65536 | tf_op jit(solution)/shard_map/all_to_all | solution.py:25
  62.1 14.8 %all_to_all.39.got = bf16[16,16,256]{2,1,0:T(8,128)(2,1)S(1)} all-to-all(bf16[16,16,256]{2,1,0:T(8,128)(2,1)S(1)} %broadcast_in_dim.3), channel_id=1, replica_groups=mesh['kv_0'=4,'kv_1'=4,'z'=16,'core'=2] {'z'}, dimensions={0} | all-to-all | bytes 262144 | tf_op jit(solution)/shard_map/all_to_all | solution.py:25
  76.9 0.0 copy-done.2
  76.9 0.0 copy-done.10
  76.9 0.2 mix.1
  77.1 10.7 %all_to_all.40.got = bf16[16,16,640]{2,1,0:T(8,128)(2,1)S(1)} all-to-all(bf16[16,16,640]{2,1,0:T(8,128)(2,1)S(1)} %get-tuple-element.17), channel_id=1, replica_groups=mesh['kv_0'=4,'kv_1'=4,'z'=16,'core'=2] {'kv_0','kv_1'}, dimensions={0} | all-to-all | bytes 655360 | tf_op jit(solution)/shard_map/all_to_all | solution.py:25
  87.8 0.0 copy-done.3
  87.8 0.5 down.1
  88.3 20.7 %all_to_all.41.got = f32[32,1,128]{2,1,0:T(1,128)S(1)} all-to-all(f32[32,1,128]{2,1,0:T(1,128)S(1)} %down.1), channel_id=1, replica_groups=mesh['kv_0'=4,'kv_1'=4,'z'=16,'core'=2] {'z','core'}, dimensions={0} | all-to-all | bytes 32768 | tf_op jit(solution)/shard_map/all_to_all | solution.py:25
  109.0 0.7 finish.1
  (10 shorter events, 0.0 us)
Async XLA Ops:
  0.0 0.7 copy-start.11
  0.7 28.6 %copy-start.1 = (bf16[32,4096]{1,0:T(8,128)(2,1)S(1)}, bf16[32,4096]{1,0:T(8,128)(2,1)}, u32[]{:S(2)}) copy-start(bf16[32,4096]{1,0:T(8,128)(2,1)} %forget_w.1) | copy-start | bytes 786436
  0.7 28.6 %copy-start.5 = (bf16[64,256]{1,0:T(8,128)(2,1)S(1)}, bf16[64,256]{1,0:T(8,128)(2,1)}, u32[]{:S(2)}) copy-start(bf16[64,256]{1,0:T(8,128)(2,1)} %query_w.1) | copy-start | bytes 98308
  0.7 28.6 %copy-start.6 = (bf16[64,256]{1,0:T(8,128)(2,1)S(1)}, bf16[64,256]{1,0:T(8,128)(2,1)}, u32[]{:S(2)}) copy-start(bf16[64,256]{1,0:T(8,128)(2,1)} %key_w.1) | copy-start | bytes 98308
  0.7 28.6 %copy-start.7 = (bf16[64,256]{1,0:T(8,128)(2,1)S(1)}, bf16[64,256]{1,0:T(8,128)(2,1)}, u32[]{:S(2)}) copy-start(bf16[64,256]{1,0:T(8,128)(2,1)} %value_w.1) | copy-start | bytes 98308
  0.7 28.6 %copy-start.9 = (bf16[4096]{0:T(1024)(128)(2,1)S(1)}, bf16[4096]{0:T(1024)(128)(2,1)}, u32[]{:S(2)}) copy-start(bf16[4096]{0:T(1024)(128)(2,1)} %param.14) | copy-start | bytes 24580
  29.3 14.2 %copy-start = (bf16[16,1,2,64,1024]{4,3,2,1,0:T(8,128)(2,1)S(1)}, bf16[16,1,2,64,1024]{4,3,2,1,0:T(8,128)(2,1)}, u32[]{:S(2)}) copy-start(bf16[16,1,2,64,1024]{4,3,2,1,0:T(8,128)(2,1)} %pairs.1) | copy-start | bytes 12582916
  29.3 14.1 %copy-start.4 = (f32[16,1,1024]{2,1,0:T(1,128)S(1)}, f32[16,1,1024]{2,1,0:T(1,128)}, u32[]{:S(2)}) copy-start(f32[16,1,1024]{2,1,0:T(1,128)} %gates.1) | copy-start | bytes 196612
  29.3 14.1 %copy-start.12 = (s32[16]{0:T(128)S(1)}, s32[16]{0:T(128)}, u32[]{:S(2)}) copy-start(s32[16]{0:T(128)} %lengths.1) | copy-start | bytes 196
  43.5 11.2 %copy-start.8 = (bf16[64,256]{1,0:T(8,128)(2,1)S(1)}, bf16[64,256]{1,0:T(8,128)(2,1)}, u32[]{:S(2)}) copy-start(bf16[64,256]{1,0:T(8,128)(2,1)} %output_w.1) | copy-start | bytes 98308
  54.7 22.2 %copy-start.2 = (bf16[512,256]{1,0:T(8,128)(2,1)S(1)}, bf16[512,256]{1,0:T(8,128)(2,1)}, u32[]{:S(2)}) copy-start(bf16[512,256]{1,0:T(8,128)(2,1)} %up_w.1) | copy-start | bytes 786436
  54.7 22.2 %copy-start.10 = (bf16[4096]{0:T(1024)(128)(2,1)S(1)}, bf16[4096]{0:T(1024)(128)(2,1)}, u32[]{:S(2)}) copy-start(bf16[4096]{0:T(1024)(128)(2,1)} %param.23) | copy-start | bytes 24580
  76.9 10.9 %copy-start.3 = (bf16[512,256]{1,0:T(8,128)(2,1)S(1)}, bf16[512,256]{1,0:T(8,128)(2,1)}, u32[]{:S(2)}) copy-start(bf16[512,256]{1,0:T(8,128)(2,1)} %down_w.1) | copy-start | bytes 786436

commit v3 on v2

--- a/solution.py
+++ b/solution.py
@@ -2,6 +2,7 @@
 
 import jax
 import jax.numpy as jnp
+import numpy as np
 from jax import lax
 from jax.experimental import pallas as pl
 from jax.experimental.pallas import tpu as pltpu
@@ -21,8 +22,19 @@
 BF16 = jnp.bfloat16
 
 
+def far_first(sizes):
+    order = np.arange(np.prod(sizes)).reshape(sizes)
+    for dim, size in enumerate(sizes):
+        if size > 2:
+            order = np.roll(order, -(size // 2), axis=dim)
+    return [[int(index) for index in order.reshape(-1)]]
+
+
 def exchange(copies, axes):
-    return lax.all_to_all(copies, axes, split_axis=0, concat_axis=0, tiled=True)
+    sizes = [lax.axis_size(axis) for axis in ((axes,) if isinstance(axes, str) else axes)]
+    return lax.all_to_all(
+        copies, axes, split_axis=0, concat_axis=0, tiled=True, axis_index_groups=far_first(sizes)
+    )
 
 
 def near(array):
@@ -68,7 +80,8 @@
     peers = got.shape[0]
     sequences = block_out.shape[0]
     columns = LANES // sequences
-    spread = jnp.broadcast_to(got[...], (peers, columns, LANES)).reshape(peers * columns, LANES)
+    lines = jnp.concatenate([got[peers // 2 :], got[: peers // 2]], axis=0)
+    spread = jnp.broadcast_to(lines, (peers, columns, LANES)).reshape(peers * columns, LANES)
     keep = (iota(spread.shape, 1) // sequences) == (iota(spread.shape, 0) % columns)
     fold = (iota((sequences, LANES), 1) % sequences) == iota((sequences, LANES), 0)
     block = rows_dot(
@@ -187,7 +200,9 @@
     peers = out.shape[0]
     columns = LANES // sequences
     lines = [turned[pl.ds(at, peers, stride=columns), :] for at in range(columns)]
-    out[...] = jnp.concatenate(lines, axis=1).reshape(out.shape)
+    lines = jnp.concatenate(lines, axis=1)
+    lines = jnp.concatenate([lines[peers // 2 :], lines[: peers // 2]], axis=0)
+    out[...] = lines.reshape(out.shape)
 
 
 def finish_body(got, middle, out):

time: 110 us -> 100 us (0.909)
  blocking collectives: 105 us -> 95.5 us
    all_to_all x7, blocking collectives: 105 us -> 95.5 us  [exchange(): lax.all_to_all(copies, axes, split_axis=0, concat_axis=0, tiled=True, axi...]
where the time goes in v3:
time: 100 us
  blocking collectives  95.5 us (96%)
  Pallas kernels  3.64 us (4%)
    all_to_all x7, blocking collectives, exchange(): lax.all_to_all(copies, axes, split_axis=0, concat_axis=0, tiled=True, axi...  95.5 us

profile of v3, /device:TPU:1, one launch (start us, length us, event | category | flops | bytes accessed | tf_op | source)
XLA Modules:
  0.0 100.0 jit_solution(12150542927720108806)
XLA Ops:
  0.0 0.7 copy-done.11
  0.7 0.0 copy-start.9
  0.7 0.1 spread.1
  0.8 22.3 %all_to_all.35.got = f32[32,1,128]{2,1,0:T(1,128)S(1)} all-to-all(f32[32,1,128]{2,1,0:T(1,128)S(1)} %spread.1), channel_id=1, replica_groups={{16,17,18,19,20,21,22,23,24,25,26,27,28,29,30,31,0,1,2,3,4,5,6,7,8,9,10..., dimensions={0} | all-to-all | bytes 32768 | tf_op jit(solution)/shard_map/all_to_all | solution.py:35
  23.1 0.0 copy-done.1
  23.1 0.0 copy-done.5
  23.1 0.0 copy-done.6
  23.1 0.0 copy-done.7
  23.1 0.0 copy-done.9
  23.1 0.0 copy-start
  23.1 0.0 copy-start.4
  23.1 0.0 copy-start.12
  23.1 0.4 project.1
  23.6 10.8 %all_to_all.36.got = f32[16,16,128]{2,1,0:T(8,128)S(1)} all-to-all(f32[16,16,128]{2,1,0:T(8,128)S(1)} %get-tuple-element.12), channel_id=1, replica_groups={{320,352,256,288,448,480,384,416,64,96,0,32,192,224,128,160},{321,353,2..., dimensions={0} | all-to-all | bytes 262144 | tf_op jit(solution)/shard_map/all_to_all | solution.py:35
  34.4 0.0 copy-done
  34.4 0.0 copy-done.4
  34.4 0.0 copy-done.12
  34.4 0.0 copy-start.8
  34.4 1.2 %attend.1 = (bf16[16,16,256]{2,1,0:T(8,128)(2,1)S(1)}, f32[16,128]{1,0:T(8,128)S(1)}) custom-call(f32[16,16,128]{2,1,0:T(8,128)S(1)} %all_to_all.36.got, f32[16,128]{1,0:T(8,128)S(1)} %get-tuple-element.13.parts, bf16[16,1,2,64,1024]{4,3,2,1,0:T(8,128)(2,1)S(1)} %copy-done, f32[16,1,1024]{2,1,0:T(1,128)S(1)} %copy-done.4, s32[16]{0:T(128)S(1)} %copy-done.12), custom_call_target="tpu_custom_call" | custom-call | flops 17179869184 | bytes 67108864 | tf_op jit(solution)/shard_map/attend/pallas_call | solution.py:257
  35.6 9.5 %all_to_all.37.got = bf16[16,16,256]{2,1,0:T(8,128)(2,1)S(1)} all-to-all(bf16[16,16,256]{2,1,0:T(8,128)(2,1)S(1)} %get-tuple-element.14), channel_id=1, replica_groups={{320,352,256,288,448,480,384,416,64,96,0,32,192,224,128,160},{321,353,2..., dimensions={0} | all-to-all | bytes 262144 | tf_op jit(solution)/shard_map/all_to_all | solution.py:35
  45.1 0.0 copy-done.8
  45.1 0.5 combine.1
  45.6 6.7 %all_to_all.38 = f32[2,16,256]{2,1,0:T(8,128)S(1)} all-to-all(f32[2,16,256]{2,1,0:T(8,128)S(1)} %combine.1), channel_id=1, replica_groups={{0,1},{2,3},{4,5},{6,7},{8,9},{10,11},{12,13},{14,15},{16,17},{18,19},{..., dimensions={0} | all-to-all | bytes 65536 | tf_op jit(solution)/shard_map/all_to_all | solution.py:35
  52.3 19.5 %all_to_all.39.got = bf16[16,16,256]{2,1,0:T(8,128)(2,1)S(1)} all-to-all(bf16[16,16,256]{2,1,0:T(8,128)(2,1)S(1)} %broadcast_in_dim.3), channel_id=1, replica_groups={{16,18,20,22,24,26,28,30,0,2,4,6,8,10,12,14},{17,19,21,23,25,27,29,31,1..., dimensions={0} | all-to-all | bytes 262144 | tf_op jit(solution)/shard_map/all_to_all | solution.py:35
  71.8 0.0 copy-done.2
  71.8 0.0 copy-done.10
  71.8 0.2 mix.1
  72.0 12.2 %all_to_all.40.got = bf16[16,16,640]{2,1,0:T(8,128)(2,1)S(1)} all-to-all(bf16[16,16,640]{2,1,0:T(8,128)(2,1)S(1)} %get-tuple-element.17), channel_id=1, replica_groups={{320,352,256,288,448,480,384,416,64,96,0,32,192,224,128,160},{321,353,2..., dimensions={0} | all-to-all | bytes 655360 | tf_op jit(solution)/shard_map/all_to_all | solution.py:35
  84.2 0.0 copy-done.3
  84.2 0.5 down.1
  84.7 14.6 %all_to_all.41.got = f32[32,1,128]{2,1,0:T(1,128)S(1)} all-to-all(f32[32,1,128]{2,1,0:T(1,128)S(1)} %down.1), channel_id=1, replica_groups={{16,17,18,19,20,21,22,23,24,25,26,27,28,29,30,31,0,1,2,3,4,5,6,7,8,9,10..., dimensions={0} | all-to-all | bytes 32768 | tf_op jit(solution)/shard_map/all_to_all | solution.py:35
  99.3 0.7 finish.1
  (10 shorter events, 0.0 us)
Async XLA Ops:
  0.0 0.7 copy-start.11
  0.7 22.4 %copy-start.1 = (bf16[32,4096]{1,0:T(8,128)(2,1)S(1)}, bf16[32,4096]{1,0:T(8,128)(2,1)}, u32[]{:S(2)}) copy-start(bf16[32,4096]{1,0:T(8,128)(2,1)} %forget_w.1) | copy-start | bytes 786436
  0.7 22.4 %copy-start.5 = (bf16[64,256]{1,0:T(8,128)(2,1)S(1)}, bf16[64,256]{1,0:T(8,128)(2,1)}, u32[]{:S(2)}) copy-start(bf16[64,256]{1,0:T(8,128)(2,1)} %query_w.1) | copy-start | bytes 98308
  0.7 22.4 %copy-start.6 = (bf16[64,256]{1,0:T(8,128)(2,1)S(1)}, bf16[64,256]{1,0:T(8,128)(2,1)}, u32[]{:S(2)}) copy-start(bf16[64,256]{1,0:T(8,128)(2,1)} %key_w.1) | copy-start | bytes 98308
  0.7 22.4 %copy-start.7 = (bf16[64,256]{1,0:T(8,128)(2,1)S(1)}, bf16[64,256]{1,0:T(8,128)(2,1)}, u32[]{:S(2)}) copy-start(bf16[64,256]{1,0:T(8,128)(2,1)} %value_w.1) | copy-start | bytes 98308
  0.7 22.4 %copy-start.9 = (bf16[4096]{0:T(1024)(128)(2,1)S(1)}, bf16[4096]{0:T(1024)(128)(2,1)}, u32[]{:S(2)}) copy-start(bf16[4096]{0:T(1024)(128)(2,1)} %param.14) | copy-start | bytes 24580
  23.1 11.3 %copy-start = (bf16[16,1,2,64,1024]{4,3,2,1,0:T(8,128)(2,1)S(1)}, bf16[16,1,2,64,1024]{4,3,2,1,0:T(8,128)(2,1)}, u32[]{:S(2)}) copy-start(bf16[16,1,2,64,1024]{4,3,2,1,0:T(8,128)(2,1)} %pairs.1) | copy-start | bytes 12582916
  23.1 11.3 %copy-start.4 = (f32[16,1,1024]{2,1,0:T(1,128)S(1)}, f32[16,1,1024]{2,1,0:T(1,128)}, u32[]{:S(2)}) copy-start(f32[16,1,1024]{2,1,0:T(1,128)} %gates.1) | copy-start | bytes 196612
  23.1 11.3 %copy-start.12 = (s32[16]{0:T(128)S(1)}, s32[16]{0:T(128)}, u32[]{:S(2)}) copy-start(s32[16]{0:T(128)} %lengths.1) | copy-start | bytes 196
  34.4 10.7 %copy-start.8 = (bf16[64,256]{1,0:T(8,128)(2,1)S(1)}, bf16[64,256]{1,0:T(8,128)(2,1)}, u32[]{:S(2)}) copy-start(bf16[64,256]{1,0:T(8,128)(2,1)} %output_w.1) | copy-start | bytes 98308
  45.1 26.7 %copy-start.2 = (bf16[512,256]{1,0:T(8,128)(2,1)S(1)}, bf16[512,256]{1,0:T(8,128)(2,1)}, u32[]{:S(2)}) copy-start(bf16[512,256]{1,0:T(8,128)(2,1)} %up_w.1) | copy-start | bytes 786436
  45.1 26.7 %copy-start.10 = (bf16[4096]{0:T(1024)(128)(2,1)S(1)}, bf16[4096]{0:T(1024)(128)(2,1)}, u32[]{:S(2)}) copy-start(bf16[4096]{0:T(1024)(128)(2,1)} %param.23) | copy-start | bytes 24580
  71.8 12.4 %copy-start.3 = (bf16[512,256]{1,0:T(8,128)(2,1)S(1)}, bf16[512,256]{1,0:T(8,128)(2,1)}, u32[]{:S(2)}) copy-start(bf16[512,256]{1,0:T(8,128)(2,1)} %down_w.1) | copy-start | bytes 786436

commit v4 on v2

--- a/solution.py
+++ b/solution.py
@@ -2,6 +2,7 @@
 
 import jax
 import jax.numpy as jnp
+import numpy as np
 from jax import lax
 from jax.experimental import pallas as pl
 from jax.experimental.pallas import tpu as pltpu
@@ -21,8 +22,23 @@
 BF16 = jnp.bfloat16
 
 
+FIRST_Z, FIRST_TP = 9, 19
+
+
+def group_of(axes):
+    if axes == KV:
+        order = np.roll(np.arange(16).reshape(4, 4), (-2, -2), (0, 1))
+    elif axes == TP:
+        order = np.roll(np.arange(32), -FIRST_TP)
+    else:
+        order = np.roll(np.arange(16), -FIRST_Z)
+    return [[int(index) for index in order.reshape(-1)]]
+
+
 def exchange(copies, axes):
-    return lax.all_to_all(copies, axes, split_axis=0, concat_axis=0, tiled=True)
+    return lax.all_to_all(
+        copies, axes, split_axis=0, concat_axis=0, tiled=True, axis_index_groups=group_of(axes)
+    )
 
 
 def near(array):
@@ -68,7 +84,8 @@
     peers = got.shape[0]
     sequences = block_out.shape[0]
     columns = LANES // sequences
-    spread = jnp.broadcast_to(got[...], (peers, columns, LANES)).reshape(peers * columns, LANES)
+    lines = jnp.concatenate([got[peers - FIRST_TP :], got[: peers - FIRST_TP]], axis=0)
+    spread = jnp.broadcast_to(lines, (peers, columns, LANES)).reshape(peers * columns, LANES)
     keep = (iota(spread.shape, 1) // sequences) == (iota(spread.shape, 0) % columns)
     fold = (iota((sequences, LANES), 1) % sequences) == iota((sequences, LANES), 0)
     block = rows_dot(
@@ -154,7 +171,7 @@
     denominator = jnp.sum(factors * stat(3), axis=0) + own_factor
     attended = (numerator / denominator).astype(BF16)
     projected = jnp.dot(attended, output_w[...], preferred_element_type=F32)
-    out[...] = jnp.broadcast_to(projected[None], out.shape)
+    out[...] = projected
 
 
 def mix_body(got, block, gain, up_w, third_out, middle_out):
@@ -166,28 +183,36 @@
     scaled = (wide * block_gain(gain, position)).astype(BF16)
     hidden = rows_dot(scaled, up_w[...])
     squares = jnp.sum(wide * wide, axis=1, keepdims=True)
-    lane = iota((wide.shape[0], LANES), 1)
-    stats = jnp.zeros(lane.shape, F32)
-    for at, piece in enumerate(pieces(squares)):
-        stats = jnp.where(lane == at, piece, stats)
-    out = jnp.concatenate([hidden, stats], axis=1).astype(BF16)
+    sequences, units = hidden.shape
+    diagonal = iota((sequences, LANES), 0) == iota((sequences, LANES), 1)
+    across = jnp.sum(jnp.where(diagonal, squares, 0.0), axis=0, keepdims=True)
+    row = iota((8, LANES), 0)
+    stats = jnp.zeros(row.shape, F32)
+    for at, piece in enumerate(pieces(across)):
+        stats = jnp.where(row == at, piece, stats)
+    parts = [hidden[:, at : at + LANES] for at in range(0, units, LANES)]
+    out = jnp.concatenate([*parts, stats], axis=0).astype(BF16)
     third_out[...] = jnp.broadcast_to(out[None], third_out.shape)
 
 
 def down_body(model_width, got, down_w, out, turned):
     summed = jnp.sum(got[...].astype(F32), axis=0)
-    units = down_w.shape[0]
-    squares = summed[:, units : units + 1] + summed[:, units + 1 : units + 2]
-    squares = squares + summed[:, units + 2 : units + 3]
+    sequences = turned.shape[1]
+    units = down_w.shape[0] // LANES * sequences
+    parts = [summed[at : at + sequences] for at in range(0, units, sequences)]
+    across = jnp.sum(summed[units : units + 3], axis=0, keepdims=True)
+    diagonal = iota((sequences, LANES), 0) == iota((sequences, LANES), 1)
+    squares = jnp.sum(jnp.where(diagonal, across, 0.0), axis=1, keepdims=True)
     scale = lax.rsqrt(squares / model_width + EPSILON)
-    activated = jnp.square(jax.nn.relu(summed[:, :units] * scale)).astype(BF16)
-    sequences = activated.shape[0]
+    activated = [jnp.square(jax.nn.relu(part * scale)).astype(BF16) for part in parts]
+    activated = jnp.concatenate(activated, axis=1)
     down = jnp.dot(activated, down_w[...], preferred_element_type=F32)
     turned[...] = down.T
     peers = out.shape[0]
     columns = LANES // sequences
     lines = [turned[pl.ds(at, peers, stride=columns), :] for at in range(columns)]
-    out[...] = jnp.concatenate(lines, axis=1).reshape(out.shape)
+    lines = jnp.concatenate(lines, axis=1).reshape(out.shape)
+    out[...] = jnp.concatenate([lines[FIRST_TP:], lines[:FIRST_TP]], axis=0)
 
 
 def finish_body(got, middle, out):
@@ -245,14 +270,15 @@
         "attend",
     )(got, parts, near(cached_pairs), near(cached_gates), near(lengths))
     got = exchange(second, KV)
-    (projected,) = call(combine_body, [((2, sequences, width), F32)], "combine")(
+    (projected,) = call(combine_body, [((sequences, width), F32)], "combine")(
         got, row, near(output_weight)
     )
-    projected = jnp.sum(exchange(projected, "core"), axis=0).astype(BF16)
+    projected = projected + lax.ppermute(projected, "core", [(0, 1), (1, 0)])
+    projected = projected.astype(BF16)
     got = exchange(jnp.broadcast_to(projected, (lax.axis_size("z"), *projected.shape)), "z")
     third, middle = call(
         mix_body,
-        [((blocks, sequences, hidden_units + LANES), BF16), ((sequences, width), BF16)],
+        [((blocks, sequences * hidden_units // LANES + 8, LANES), BF16), ((sequences, width), BF16)],
         "mix",
     )(got, block, near(mixer_gain.reshape(-1, LANES)), near(up_weight))
     got = exchange(third, KV)

time: 110 us -> 98.7 us (0.90)
  blocking collectives: 105 us -> 87.8 us
  starting transfers between devices: 0 us -> 5.21 us
    all_to_all x7 -> x6, blocking collectives: 105 us -> 87.8 us  [exchange(): lax.all_to_all(copies, axes, split_axis=0, concat_axis=0, tiled=True, axi...]
    ppermute x0 -> x1, starting transfers between devices: none -> 5.21 us  [local(): projected = projected + lax.ppermute(projected, 'core', [(0, 1), (1, 0)])]
  transfers between devices with their start and end apart: 0 -> 1, of which waited for: 0 -> 1; matrix products, arithmetic and copies ran while one was open for 0% -> 0% of each run, Pallas kernels for 0% -> 0%
where the time goes in v4:
time: 98.7 us; the launch traced here: 98.3 us
  blocking collectives  87.8 us (89%)
  starting transfers between devices  5.21 us (5%)
  Pallas kernels  3.59 us (4%)
    all_to_all x6, blocking collectives, exchange(): lax.all_to_all(copies, axes, split_axis=0, concat_axis=0, tiled=True, axi...  87.8 us
    ppermute x1, starting transfers between devices, local(): projected = projected + lax.ppermute(projected, 'core', [(0, 1), (1, 0)])  5.21 us
  transfers between devices with their start and end apart: 1, of which 1 were waited for; matrix products, arithmetic and copies ran while one was open for 0% of the time, Pallas kernels for 0%

profile of v4, /device:TPU:1, one launch (start us, length us, event | category | flops | bytes accessed | tf_op | source)
XLA Modules:
  0.0 98.3 jit_solution(11193900876753638672)
XLA Ops:
  0.0 0.7 copy-done.11
  0.7 0.0 copy-start.9
  0.7 0.1 spread.1
  0.8 21.9 %all_to_all.30.got = f32[32,1,128]{2,1,0:T(1,128)S(1)} all-to-all(f32[32,1,128]{2,1,0:T(1,128)S(1)} %spread.1), channel_id=1, replica_groups={{19,20,21,22,23,24,25,26,27,28,29,30,31,0,1,2,3,4,5,6,7,8,9,10,11,12,13..., dimensions={0} | all-to-all | bytes 32768 | tf_op jit(solution)/shard_map/all_to_all | solution.py:39
  22.7 0.0 copy-done.1
  22.7 0.0 copy-done.5
  22.7 0.0 copy-done.6
  22.7 0.0 copy-done.7
  22.7 0.0 copy-done.9
  22.8 0.0 copy-start
  22.8 0.0 copy-start.4
  22.8 0.0 copy-start.12
  22.8 0.4 project.1
  23.2 10.8 %all_to_all.31.got = f32[16,16,128]{2,1,0:T(8,128)S(1)} all-to-all(f32[16,16,128]{2,1,0:T(8,128)S(1)} %get-tuple-element.12), channel_id=1, replica_groups={{320,352,256,288,448,480,384,416,64,96,0,32,192,224,128,160},{321,353,2..., dimensions={0} | all-to-all | bytes 262144 | tf_op jit(solution)/shard_map/all_to_all | solution.py:39
  34.0 0.0 copy-done
  34.0 0.0 copy-done.4
  34.0 0.0 copy-done.12
  34.0 0.0 copy-start.8
  34.1 1.2 %attend.1 = (bf16[16,16,256]{2,1,0:T(8,128)(2,1)S(1)}, f32[16,128]{1,0:T(8,128)S(1)}) custom-call(f32[16,16,128]{2,1,0:T(8,128)S(1)} %all_to_all.31.got, f32[16,128]{1,0:T(8,128)S(1)} %get-tuple-element.13.parts, bf16[16,1,2,64,1024]{4,3,2,1,0:T(8,128)(2,1)S(1)} %copy-done, f32[16,1,1024]{2,1,0:T(1,128)S(1)} %copy-done.4, s32[16]{0:T(128)S(1)} %copy-done.12), custom_call_target="tpu_custom_call" | custom-call | flops 17179869184 | bytes 67108864 | tf_op jit(solution)/shard_map/attend/pallas_call | solution.py:267
  35.3 9.5 %all_to_all.32.got = bf16[16,16,256]{2,1,0:T(8,128)(2,1)S(1)} all-to-all(bf16[16,16,256]{2,1,0:T(8,128)(2,1)S(1)} %get-tuple-element.14), channel_id=1, replica_groups={{320,352,256,288,448,480,384,416,64,96,0,32,192,224,128,160},{321,353,2..., dimensions={0} | all-to-all | bytes 262144 | tf_op jit(solution)/shard_map/all_to_all | solution.py:39
  44.8 0.0 copy-done.8
  44.8 0.5 combine.1
  45.3 5.2 %collective-permute-start = (f32[16,256]{1,0:T(8,128)S(1)}, f32[16,256]{1,0:T(8,128)S(1)}, u32[]{:S(2)}, u32[]{:S(2)}) collective-permute-start(f32[16,256]{1,0:T(8,128)S(1)} %combine.1), channel_id=1, source_target_pairs={{0,1},{1,0},{2,3},{3,2},{4,5},{5,4},{6,7},{7,6},{8,9},{9,8},{10,11... | collective-permute-start | bytes 49160 | tf_op jit(solution)/shard_map/ppermute | solution.py:276
  50.5 0.8 collective-permute-done
  51.4 19.5 %all_to_all.33.got = bf16[16,16,256]{2,1,0:T(8,128)(2,1)S(1)} all-to-all(bf16[16,16,256]{2,1,0:T(8,128)(2,1)S(1)} %broadcast_in_dim.3), channel_id=1, replica_groups={{18,20,22,24,26,28,30,0,2,4,6,8,10,12,14,16},{19,21,23,25,27,29,31,1,3,..., dimensions={0} | all-to-all | bytes 262144 | tf_op jit(solution)/shard_map/all_to_all | solution.py:39
  70.9 0.0 copy-done.2
  70.9 0.0 copy-done.10
  70.9 0.2 mix.1
  71.1 11.8 %all_to_all.34.got = bf16[16,72,128]{2,1,0:T(8,128)(2,1)S(1)} all-to-all(bf16[16,72,128]{2,1,0:T(8,128)(2,1)S(1)} %get-tuple-element.17), channel_id=1, replica_groups={{320,352,256,288,448,480,384,416,64,96,0,32,192,224,128,160},{321,353,2..., dimensions={0} | all-to-all | bytes 589824 | tf_op jit(solution)/shard_map/all_to_all | solution.py:39
  82.9 0.4 down.1
  83.4 14.3 %all_to_all.35.got = f32[32,1,128]{2,1,0:T(1,128)S(1)} all-to-all(f32[32,1,128]{2,1,0:T(1,128)S(1)} %down.1), channel_id=1, replica_groups={{19,20,21,22,23,24,25,26,27,28,29,30,31,0,1,2,3,4,5,6,7,8,9,10,11,12,13..., dimensions={0} | all-to-all | bytes 32768 | tf_op jit(solution)/shard_map/all_to_all | solution.py:39
  97.6 0.7 finish.1
  (11 shorter events, 0.0 us)
Async XLA Ops:
  0.0 0.7 copy-start.11
  0.7 22.0 %copy-start.1 = (bf16[32,4096]{1,0:T(8,128)(2,1)S(1)}, bf16[32,4096]{1,0:T(8,128)(2,1)}, u32[]{:S(2)}) copy-start(bf16[32,4096]{1,0:T(8,128)(2,1)} %forget_w.1) | copy-start | bytes 786436
  0.7 22.0 %copy-start.5 = (bf16[64,256]{1,0:T(8,128)(2,1)S(1)}, bf16[64,256]{1,0:T(8,128)(2,1)}, u32[]{:S(2)}) copy-start(bf16[64,256]{1,0:T(8,128)(2,1)} %query_w.1) | copy-start | bytes 98308
  0.7 22.0 %copy-start.6 = (bf16[64,256]{1,0:T(8,128)(2,1)S(1)}, bf16[64,256]{1,0:T(8,128)(2,1)}, u32[]{:S(2)}) copy-start(bf16[64,256]{1,0:T(8,128)(2,1)} %key_w.1) | copy-start | bytes 98308
  0.7 22.0 %copy-start.7 = (bf16[64,256]{1,0:T(8,128)(2,1)S(1)}, bf16[64,256]{1,0:T(8,128)(2,1)}, u32[]{:S(2)}) copy-start(bf16[64,256]{1,0:T(8,128)(2,1)} %value_w.1) | copy-start | bytes 98308
  0.7 22.1 %copy-start.9 = (bf16[4096]{0:T(1024)(128)(2,1)S(1)}, bf16[4096]{0:T(1024)(128)(2,1)}, u32[]{:S(2)}) copy-start(bf16[4096]{0:T(1024)(128)(2,1)} %param.14) | copy-start | bytes 24580
  22.8 11.3 %copy-start = (bf16[16,1,2,64,1024]{4,3,2,1,0:T(8,128)(2,1)S(1)}, bf16[16,1,2,64,1024]{4,3,2,1,0:T(8,128)(2,1)}, u32[]{:S(2)}) copy-start(bf16[16,1,2,64,1024]{4,3,2,1,0:T(8,128)(2,1)} %pairs.1) | copy-start | bytes 12582916
  22.8 11.3 %copy-start.4 = (f32[16,1,1024]{2,1,0:T(1,128)S(1)}, f32[16,1,1024]{2,1,0:T(1,128)}, u32[]{:S(2)}) copy-start(f32[16,1,1024]{2,1,0:T(1,128)} %gates.1) | copy-start | bytes 196612
  22.8 11.3 %copy-start.12 = (s32[16]{0:T(128)S(1)}, s32[16]{0:T(128)}, u32[]{:S(2)}) copy-start(s32[16]{0:T(128)} %lengths.1) | copy-start | bytes 196
  34.0 10.7 %copy-start.8 = (bf16[64,256]{1,0:T(8,128)(2,1)S(1)}, bf16[64,256]{1,0:T(8,128)(2,1)}, u32[]{:S(2)}) copy-start(bf16[64,256]{1,0:T(8,128)(2,1)} %output_w.1) | copy-start | bytes 98308
  44.8 26.1 %copy-start.2 = (bf16[512,256]{1,0:T(8,128)(2,1)S(1)}, bf16[512,256]{1,0:T(8,128)(2,1)}, u32[]{:S(2)}) copy-start(bf16[512,256]{1,0:T(8,128)(2,1)} %up_w.1) | copy-start | bytes 786436
  44.8 26.1 %copy-start.10 = (bf16[4096]{0:T(1024)(128)(2,1)S(1)}, bf16[4096]{0:T(1024)(128)(2,1)}, u32[]{:S(2)}) copy-start(bf16[4096]{0:T(1024)(128)(2,1)} %param.23) | copy-start | bytes 24580
  45.3 6.0 %collective-permute-start = (f32[16,256]{1,0:T(8,128)S(1)}, f32[16,256]{1,0:T(8,128)S(1)}, u32[]{:S(2)}, u32[]{:S(2)}) collective-permute-start(f32[16,256]{1,0:T(8,128)S(1)} %combine.1), channel_id=1, source_target_pairs={{0,1},{1,0},{2,3},{3,2},{4,5},{5,4},{6,7},{7,6},{8,9},{9,8},{10,11... | collective-permute-start | bytes 49160 | tf_op jit(solution)/shard_map/ppermute | solution.py:276
  70.9 12.0 %copy-start.3 = (bf16[512,256]{1,0:T(8,128)(2,1)S(1)}, bf16[512,256]{1,0:T(8,128)(2,1)}, u32[]{:S(2)}) copy-start(bf16[512,256]{1,0:T(8,128)(2,1)} %down_w.1) | copy-start | bytes 786436

commit v5 on v4

--- a/solution.py
+++ b/solution.py
@@ -27,11 +27,12 @@
 
 def group_of(axes):
     if axes == KV:
-        order = np.roll(np.arange(16).reshape(4, 4), (-2, -2), (0, 1))
+        row, column = np.divmod(np.arange(16), 4)
+        order = (row + 2 * column + 2) % 4 * 4 + (column + 2) % 4
     elif axes == TP:
         order = np.roll(np.arange(32), -FIRST_TP)
     else:
-        order = np.roll(np.arange(16), -FIRST_Z)
+        order = (FIRST_Z + 7 * np.arange(16)) % 16
     return [[int(index) for index in order.reshape(-1)]]
 
 

time: 98.7 us -> 98.2 us (level)
  no operation moved by 1% of the time
where the time goes in v5:
time: 98.2 us; the launch traced here: 97.8 us
  blocking collectives  87.4 us (89%)
  starting transfers between devices  5.17 us (5%)
  Pallas kernels  3.59 us (4%)
    all_to_all x6, blocking collectives, exchange(): lax.all_to_all(copies, axes, split_axis=0, concat_axis=0, tiled=True, axi...  87.4 us
    ppermute x1, starting transfers between devices, local(): projected = projected + lax.ppermute(projected, 'core', [(0, 1), (1, 0)])  5.17 us
  transfers between devices with their start and end apart: 1, of which 1 were waited for; matrix products, arithmetic and copies ran while one was open for 0% of the time, Pallas kernels for 0%

profile of v5, /device:TPU:1, one launch (start us, length us, event | category | flops | bytes accessed | tf_op | source)
XLA Modules:
  0.0 97.8 jit_solution(979973873770702743)
XLA Ops:
  0.0 0.7 copy-done.11
  0.7 0.0 copy-start.9
  0.7 0.1 spread.1
  0.8 21.9 %all_to_all.30.got = f32[32,1,128]{2,1,0:T(1,128)S(1)} all-to-all(f32[32,1,128]{2,1,0:T(1,128)S(1)} %spread.1), channel_id=1, replica_groups={{19,20,21,22,23,24,25,26,27,28,29,30,31,0,1,2,3,4,5,6,7,8,9,10,11,12,13..., dimensions={0} | all-to-all | bytes 32768 | tf_op jit(solution)/shard_map/all_to_all | solution.py:40
  22.7 0.0 copy-done.1
  22.7 0.0 copy-done.5
  22.7 0.0 copy-done.6
  22.7 0.0 copy-done.7
  22.7 0.0 copy-done.9
  22.8 0.0 copy-start
  22.8 0.0 copy-start.4
  22.8 0.0 copy-start.12
  22.8 0.4 project.1
  23.2 10.8 %all_to_all.31.got = f32[16,16,128]{2,1,0:T(8,128)S(1)} all-to-all(f32[16,16,128]{2,1,0:T(8,128)S(1)} %get-tuple-element.12), channel_id=1, replica_groups={{320,96,256,32,448,224,384,160,64,352,0,288,192,480,128,416},{321,97,25..., dimensions={0} | all-to-all | bytes 262144 | tf_op jit(solution)/shard_map/all_to_all | solution.py:40
  34.0 0.0 copy-done
  34.0 0.0 copy-done.4
  34.0 0.0 copy-done.12
  34.0 0.0 copy-start.8
  34.1 1.2 %attend.1 = (bf16[16,16,256]{2,1,0:T(8,128)(2,1)S(1)}, f32[16,128]{1,0:T(8,128)S(1)}) custom-call(f32[16,16,128]{2,1,0:T(8,128)S(1)} %all_to_all.31.got, f32[16,128]{1,0:T(8,128)S(1)} %get-tuple-element.13.parts, bf16[16,1,2,64,1024]{4,3,2,1,0:T(8,128)(2,1)S(1)} %copy-done, f32[16,1,1024]{2,1,0:T(1,128)S(1)} %copy-done.4, s32[16]{0:T(128)S(1)} %copy-done.12), custom_call_target="tpu_custom_call" | custom-call | flops 17179869184 | bytes 67108864 | tf_op jit(solution)/shard_map/attend/pallas_call | solution.py:268
  35.3 9.4 %all_to_all.32.got = bf16[16,16,256]{2,1,0:T(8,128)(2,1)S(1)} all-to-all(bf16[16,16,256]{2,1,0:T(8,128)(2,1)S(1)} %get-tuple-element.14), channel_id=1, replica_groups={{320,96,256,32,448,224,384,160,64,352,0,288,192,480,128,416},{321,97,25..., dimensions={0} | all-to-all | bytes 262144 | tf_op jit(solution)/shard_map/all_to_all | solution.py:40
  44.7 0.0 copy-done.8
  44.7 0.5 combine.1
  45.2 5.2 %collective-permute-start = (f32[16,256]{1,0:T(8,128)S(1)}, f32[16,256]{1,0:T(8,128)S(1)}, u32[]{:S(2)}, u32[]{:S(2)}) collective-permute-start(f32[16,256]{1,0:T(8,128)S(1)} %combine.1), channel_id=1, source_target_pairs={{0,1},{1,0},{2,3},{3,2},{4,5},{5,4},{6,7},{7,6},{8,9},{9,8},{10,11... | collective-permute-start | bytes 49160 | tf_op jit(solution)/shard_map/ppermute | solution.py:277
  50.4 0.8 collective-permute-done
  51.2 18.8 %all_to_all.33.got = bf16[16,16,256]{2,1,0:T(8,128)(2,1)S(1)} all-to-all(bf16[16,16,256]{2,1,0:T(8,128)(2,1)S(1)} %broadcast_in_dim.3), channel_id=1, replica_groups={{18,0,14,28,10,24,6,20,2,16,30,12,26,8,22,4},{19,1,15,29,11,25,7,21,3,1..., dimensions={0} | all-to-all | bytes 262144 | tf_op jit(solution)/shard_map/all_to_all | solution.py:40
  70.0 0.0 copy-done.2
  70.0 0.0 copy-done.10
  70.0 0.2 mix.1
  70.2 10.4 %all_to_all.34.got = bf16[16,72,128]{2,1,0:T(8,128)(2,1)S(1)} all-to-all(bf16[16,72,128]{2,1,0:T(8,128)(2,1)S(1)} %get-tuple-element.17), channel_id=1, replica_groups={{320,96,256,32,448,224,384,160,64,352,0,288,192,480,128,416},{321,97,25..., dimensions={0} | all-to-all | bytes 589824 | tf_op jit(solution)/shard_map/all_to_all | solution.py:40
  80.6 0.4 down.1
  81.1 16.1 %all_to_all.35.got = f32[32,1,128]{2,1,0:T(1,128)S(1)} all-to-all(f32[32,1,128]{2,1,0:T(1,128)S(1)} %down.1), channel_id=1, replica_groups={{19,20,21,22,23,24,25,26,27,28,29,30,31,0,1,2,3,4,5,6,7,8,9,10,11,12,13..., dimensions={0} | all-to-all | bytes 32768 | tf_op jit(solution)/shard_map/all_to_all | solution.py:40
  97.1 0.7 finish.1
  (11 shorter events, 0.0 us)
Async XLA Ops:
  0.0 0.7 copy-start.11
  0.7 22.0 %copy-start.1 = (bf16[32,4096]{1,0:T(8,128)(2,1)S(1)}, bf16[32,4096]{1,0:T(8,128)(2,1)}, u32[]{:S(2)}) copy-start(bf16[32,4096]{1,0:T(8,128)(2,1)} %forget_w.1) | copy-start | bytes 786436
  0.7 22.0 %copy-start.5 = (bf16[64,256]{1,0:T(8,128)(2,1)S(1)}, bf16[64,256]{1,0:T(8,128)(2,1)}, u32[]{:S(2)}) copy-start(bf16[64,256]{1,0:T(8,128)(2,1)} %query_w.1) | copy-start | bytes 98308
  0.7 22.0 %copy-start.6 = (bf16[64,256]{1,0:T(8,128)(2,1)S(1)}, bf16[64,256]{1,0:T(8,128)(2,1)}, u32[]{:S(2)}) copy-start(bf16[64,256]{1,0:T(8,128)(2,1)} %key_w.1) | copy-start | bytes 98308
  0.7 22.0 %copy-start.7 = (bf16[64,256]{1,0:T(8,128)(2,1)S(1)}, bf16[64,256]{1,0:T(8,128)(2,1)}, u32[]{:S(2)}) copy-start(bf16[64,256]{1,0:T(8,128)(2,1)} %value_w.1) | copy-start | bytes 98308
  0.7 22.1 %copy-start.9 = (bf16[4096]{0:T(1024)(128)(2,1)S(1)}, bf16[4096]{0:T(1024)(128)(2,1)}, u32[]{:S(2)}) copy-start(bf16[4096]{0:T(1024)(128)(2,1)} %param.14) | copy-start | bytes 24580
  22.8 11.3 %copy-start = (bf16[16,1,2,64,1024]{4,3,2,1,0:T(8,128)(2,1)S(1)}, bf16[16,1,2,64,1024]{4,3,2,1,0:T(8,128)(2,1)}, u32[]{:S(2)}) copy-start(bf16[16,1,2,64,1024]{4,3,2,1,0:T(8,128)(2,1)} %pairs.1) | copy-start | bytes 12582916
  22.8 11.3 %copy-start.4 = (f32[16,1,1024]{2,1,0:T(1,128)S(1)}, f32[16,1,1024]{2,1,0:T(1,128)}, u32[]{:S(2)}) copy-start(f32[16,1,1024]{2,1,0:T(1,128)} %gates.1) | copy-start | bytes 196612
  22.8 11.3 %copy-start.12 = (s32[16]{0:T(128)S(1)}, s32[16]{0:T(128)}, u32[]{:S(2)}) copy-start(s32[16]{0:T(128)} %lengths.1) | copy-start | bytes 196
  34.0 10.6 %copy-start.8 = (bf16[64,256]{1,0:T(8,128)(2,1)S(1)}, bf16[64,256]{1,0:T(8,128)(2,1)}, u32[]{:S(2)}) copy-start(bf16[64,256]{1,0:T(8,128)(2,1)} %output_w.1) | copy-start | bytes 98308
  44.7 25.4 %copy-start.2 = (bf16[512,256]{1,0:T(8,128)(2,1)S(1)}, bf16[512,256]{1,0:T(8,128)(2,1)}, u32[]{:S(2)}) copy-start(bf16[512,256]{1,0:T(8,128)(2,1)} %up_w.1) | copy-start | bytes 786436
  44.7 25.4 %copy-start.10 = (bf16[4096]{0:T(1024)(128)(2,1)S(1)}, bf16[4096]{0:T(1024)(128)(2,1)}, u32[]{:S(2)}) copy-start(bf16[4096]{0:T(1024)(128)(2,1)} %param.23) | copy-start | bytes 24580
  45.2 6.0 %collective-permute-start = (f32[16,256]{1,0:T(8,128)S(1)}, f32[16,256]{1,0:T(8,128)S(1)}, u32[]{:S(2)}, u32[]{:S(2)}) collective-permute-start(f32[16,256]{1,0:T(8,128)S(1)} %combine.1), channel_id=1, source_target_pairs={{0,1},{1,0},{2,3},{3,2},{4,5},{5,4},{6,7},{7,6},{8,9},{9,8},{10,11... | collective-permute-start | bytes 49160 | tf_op jit(solution)/shard_map/ppermute | solution.py:277
  70.0 10.6 %copy-start.3 = (bf16[512,256]{1,0:T(8,128)(2,1)S(1)}, bf16[512,256]{1,0:T(8,128)(2,1)}, u32[]{:S(2)}) copy-start(bf16[512,256]{1,0:T(8,128)(2,1)} %down_w.1) | copy-start | bytes 786436

commit v6 on v5

--- a/solution.py
+++ b/solution.py
@@ -172,13 +172,12 @@
     denominator = jnp.sum(factors * stat(3), axis=0) + own_factor
     attended = (numerator / denominator).astype(BF16)
     projected = jnp.dot(attended, output_w[...], preferred_element_type=F32)
-    out[...] = projected
-
-
-def mix_body(got, block, gain, up_w, third_out, middle_out):
+    out[...] = jnp.broadcast_to(projected.astype(BF16)[None], out.shape)
+
+
+def mix_body(own, other, block, gain, up_w, third_out, middle_out):
     position = lax.axis_index("kv_0") * 4 + lax.axis_index("kv_1")
-    projected = jnp.sum(got[...].astype(F32), axis=0)
-    middle = (block[...] + projected).astype(BF16)
+    middle = (block[...] + (own[...] + other[...])).astype(BF16)
     middle_out[...] = middle
     wide = middle.astype(F32)
     scaled = (wide * block_gain(gain, position)).astype(BF16)
@@ -271,17 +270,16 @@
         "attend",
     )(got, parts, near(cached_pairs), near(cached_gates), near(lengths))
     got = exchange(second, KV)
-    (projected,) = call(combine_body, [((sequences, width), F32)], "combine")(
-        got, row, near(output_weight)
-    )
-    projected = projected + lax.ppermute(projected, "core", [(0, 1), (1, 0)])
-    projected = projected.astype(BF16)
-    got = exchange(jnp.broadcast_to(projected, (lax.axis_size("z"), *projected.shape)), "z")
+    (projected,) = call(
+        combine_body, [((lax.axis_size("z"), sequences, width), BF16)], "combine"
+    )(got, row, near(output_weight))
+    own = jnp.sum(exchange(projected, "z").astype(F32), axis=0)
+    other = lax.ppermute(own, "core", [(0, 1), (1, 0)])
     third, middle = call(
         mix_body,
         [((blocks, sequences * hidden_units // LANES + 8, LANES), BF16), ((sequences, width), BF16)],
         "mix",
-    )(got, block, near(mixer_gain.reshape(-1, LANES)), near(up_weight))
+    )(own, other, block, near(mixer_gain.reshape(-1, LANES)), near(up_weight))
     got = exchange(third, KV)
     (down,) = call(
         functools.partial(down_body, model_width),

time: 98.2 us -> 96.5 us (0.983)
  blocking collectives: 87.4 us -> 84.5 us
  starting transfers between devices: 5.17 us -> 6.35 us
    all_to_all x6, blocking collectives: 87.4 us -> 84.5 us  [exchange(): lax.all_to_all(copies, axes, split_axis=0, concat_axis=0, tiled=True, axi...]
    ppermute x1, starting transfers between devices: 5.17 us -> 6.35 us  [local(): other = lax.ppermute(own, 'core', [(0, 1), (1, 0)])]
where the time goes in v6:
time: 96.5 us; the launch traced here: 96.1 us
  blocking collectives  84.5 us (88%)
  starting transfers between devices  6.35 us (7%)
  Pallas kernels  3.6 us (4%)
    all_to_all x6, blocking collectives, exchange(): lax.all_to_all(copies, axes, split_axis=0, concat_axis=0, tiled=True, axi...  84.5 us
    ppermute x1, starting transfers between devices, local(): other = lax.ppermute(own, 'core', [(0, 1), (1, 0)])  6.35 us
  transfers between devices with their start and end apart: 1, of which 1 were waited for; matrix products, arithmetic and copies ran while one was open for 0% of the time, Pallas kernels for 0%

profile of v6, /device:TPU:1, one launch (start us, length us, event | category | flops | bytes accessed | tf_op | source)
XLA Modules:
  0.0 96.1 jit_solution(11455471345479687618)
XLA Ops:
  0.0 0.7 copy-done.11
  0.7 0.0 copy-start.9
  0.7 0.1 spread.1
  0.8 21.9 %all_to_all.30.got = f32[32,1,128]{2,1,0:T(1,128)S(1)} all-to-all(f32[32,1,128]{2,1,0:T(1,128)S(1)} %spread.1), channel_id=1, replica_groups={{19,20,21,22,23,24,25,26,27,28,29,30,31,0,1,2,3,4,5,6,7,8,9,10,11,12,13..., dimensions={0} | all-to-all | bytes 32768 | tf_op jit(solution)/shard_map/all_to_all | solution.py:40
  22.7 0.0 copy-done.1
  22.7 0.0 copy-done.5
  22.7 0.0 copy-done.6
  22.7 0.0 copy-done.7
  22.7 0.0 copy-done.9
  22.8 0.0 copy-start
  22.8 0.0 copy-start.4
  22.8 0.0 copy-start.12
  22.8 0.4 project.1
  23.2 10.8 %all_to_all.31.got = f32[16,16,128]{2,1,0:T(8,128)S(1)} all-to-all(f32[16,16,128]{2,1,0:T(8,128)S(1)} %get-tuple-element.12), channel_id=1, replica_groups={{320,96,256,32,448,224,384,160,64,352,0,288,192,480,128,416},{321,97,25..., dimensions={0} | all-to-all | bytes 262144 | tf_op jit(solution)/shard_map/all_to_all | solution.py:40
  34.0 0.0 copy-done
  34.0 0.0 copy-done.4
  34.0 0.0 copy-done.12
  34.0 0.0 copy-start.8
  34.1 1.2 %attend.1 = (bf16[16,16,256]{2,1,0:T(8,128)(2,1)S(1)}, f32[16,128]{1,0:T(8,128)S(1)}) custom-call(f32[16,16,128]{2,1,0:T(8,128)S(1)} %all_to_all.31.got, f32[16,128]{1,0:T(8,128)S(1)} %get-tuple-element.13.parts, bf16[16,1,2,64,1024]{4,3,2,1,0:T(8,128)(2,1)S(1)} %copy-done, f32[16,1,1024]{2,1,0:T(1,128)S(1)} %copy-done.4, s32[16]{0:T(128)S(1)} %copy-done.12), custom_call_target="tpu_custom_call" | custom-call | flops 17179869184 | bytes 67108864 | tf_op jit(solution)/shard_map/attend/pallas_call | solution.py:267
  35.3 9.4 %all_to_all.32.got = bf16[16,16,256]{2,1,0:T(8,128)(2,1)S(1)} all-to-all(bf16[16,16,256]{2,1,0:T(8,128)(2,1)S(1)} %get-tuple-element.14), channel_id=1, replica_groups={{320,96,256,32,448,224,384,160,64,352,0,288,192,480,128,416},{321,97,25..., dimensions={0} | all-to-all | bytes 262144 | tf_op jit(solution)/shard_map/all_to_all | solution.py:40
  44.7 0.0 copy-done.8
  44.7 0.5 combine.1
  45.2 16.4 %all_to_all.33 = bf16[16,16,256]{2,1,0:T(8,128)(2,1)S(1)} all-to-all(bf16[16,16,256]{2,1,0:T(8,128)(2,1)S(1)} %combine.1), channel_id=1, replica_groups={{18,0,14,28,10,24,6,20,2,16,30,12,26,8,22,4},{19,1,15,29,11,25,7,21,3,1..., dimensions={0} | all-to-all | bytes 262144 | tf_op jit(solution)/shard_map/all_to_all | solution.py:40
  61.6 6.3 %collective-permute-start = (f32[16,256]{1,0:T(8,128)S(1)}, f32[16,256]{1,0:T(8,128)S(1)}, u32[]{:S(2)}, u32[]{:S(2)}) collective-permute-start(f32[16,256]{1,0:T(8,128)S(1)} %convert_reduce_fusion.own), channel_id=1, source_target_pairs={{0,1},{1,0},{2,3},{3,2},{4,5},{5,4},{6,7},{7,6},{8,9},{9,8},{10,11... | collective-permute-start | bytes 49160 | tf_op jit(solution)/shard_map/ppermute | solution.py:277
  68.0 0.8 collective-permute-done.other
  68.8 0.0 copy-done.2
  68.8 0.0 copy-done.10
  68.8 0.2 mix.1
  69.0 11.3 %all_to_all.34.got = bf16[16,72,128]{2,1,0:T(8,128)(2,1)S(1)} all-to-all(bf16[16,72,128]{2,1,0:T(8,128)(2,1)S(1)} %get-tuple-element.17), channel_id=1, replica_groups={{320,96,256,32,448,224,384,160,64,352,0,288,192,480,128,416},{321,97,25..., dimensions={0} | all-to-all | bytes 589824 | tf_op jit(solution)/shard_map/all_to_all | solution.py:40
  80.3 0.4 down.1
  80.7 14.7 %all_to_all.35.got = f32[32,1,128]{2,1,0:T(1,128)S(1)} all-to-all(f32[32,1,128]{2,1,0:T(1,128)S(1)} %down.1), channel_id=1, replica_groups={{19,20,21,22,23,24,25,26,27,28,29,30,31,0,1,2,3,4,5,6,7,8,9,10,11,12,13..., dimensions={0} | all-to-all | bytes 32768 | tf_op jit(solution)/shard_map/all_to_all | solution.py:40
  95.4 0.7 finish.1
  (10 shorter events, 0.0 us)
Async XLA Ops:
  0.0 0.7 copy-start.11
  0.7 22.0 %copy-start.1 = (bf16[32,4096]{1,0:T(8,128)(2,1)S(1)}, bf16[32,4096]{1,0:T(8,128)(2,1)}, u32[]{:S(2)}) copy-start(bf16[32,4096]{1,0:T(8,128)(2,1)} %forget_w.1) | copy-start | bytes 786436
  0.7 22.0 %copy-start.5 = (bf16[64,256]{1,0:T(8,128)(2,1)S(1)}, bf16[64,256]{1,0:T(8,128)(2,1)}, u32[]{:S(2)}) copy-start(bf16[64,256]{1,0:T(8,128)(2,1)} %query_w.1) | copy-start | bytes 98308
  0.7 22.0 %copy-start.6 = (bf16[64,256]{1,0:T(8,128)(2,1)S(1)}, bf16[64,256]{1,0:T(8,128)(2,1)}, u32[]{:S(2)}) copy-start(bf16[64,256]{1,0:T(8,128)(2,1)} %key_w.1) | copy-start | bytes 98308
  0.7 22.0 %copy-start.7 = (bf16[64,256]{1,0:T(8,128)(2,1)S(1)}, bf16[64,256]{1,0:T(8,128)(2,1)}, u32[]{:S(2)}) copy-start(bf16[64,256]{1,0:T(8,128)(2,1)} %value_w.1) | copy-start | bytes 98308
  0.7 22.1 %copy-start.9 = (bf16[4096]{0:T(1024)(128)(2,1)S(1)}, bf16[4096]{0:T(1024)(128)(2,1)}, u32[]{:S(2)}) copy-start(bf16[4096]{0:T(1024)(128)(2,1)} %param.14) | copy-start | bytes 24580
  22.8 11.3 %copy-start = (bf16[16,1,2,64,1024]{4,3,2,1,0:T(8,128)(2,1)S(1)}, bf16[16,1,2,64,1024]{4,3,2,1,0:T(8,128)(2,1)}, u32[]{:S(2)}) copy-start(bf16[16,1,2,64,1024]{4,3,2,1,0:T(8,128)(2,1)} %pairs.1) | copy-start | bytes 12582916
  22.8 11.3 %copy-start.4 = (f32[16,1,1024]{2,1,0:T(1,128)S(1)}, f32[16,1,1024]{2,1,0:T(1,128)}, u32[]{:S(2)}) copy-start(f32[16,1,1024]{2,1,0:T(1,128)} %gates.1) | copy-start | bytes 196612
  22.8 11.3 %copy-start.12 = (s32[16]{0:T(128)S(1)}, s32[16]{0:T(128)}, u32[]{:S(2)}) copy-start(s32[16]{0:T(128)} %lengths.1) | copy-start | bytes 196
  34.0 10.6 %copy-start.8 = (bf16[64,256]{1,0:T(8,128)(2,1)S(1)}, bf16[64,256]{1,0:T(8,128)(2,1)}, u32[]{:S(2)}) copy-start(bf16[64,256]{1,0:T(8,128)(2,1)} %output_w.1) | copy-start | bytes 98308
  44.7 24.1 %copy-start.2 = (bf16[512,256]{1,0:T(8,128)(2,1)S(1)}, bf16[512,256]{1,0:T(8,128)(2,1)}, u32[]{:S(2)}) copy-start(bf16[512,256]{1,0:T(8,128)(2,1)} %up_w.1) | copy-start | bytes 786436
  44.7 24.1 %copy-start.10 = (bf16[4096]{0:T(1024)(128)(2,1)S(1)}, bf16[4096]{0:T(1024)(128)(2,1)}, u32[]{:S(2)}) copy-start(bf16[4096]{0:T(1024)(128)(2,1)} %param.23) | copy-start | bytes 24580
  61.6 7.2 %collective-permute-start = (f32[16,256]{1,0:T(8,128)S(1)}, f32[16,256]{1,0:T(8,128)S(1)}, u32[]{:S(2)}, u32[]{:S(2)}) collective-permute-start(f32[16,256]{1,0:T(8,128)S(1)} %convert_reduce_fusion.own), channel_id=1, source_target_pairs={{0,1},{1,0},{2,3},{3,2},{4,5},{5,4},{6,7},{7,6},{8,9},{9,8},{10,11... | collective-permute-start | bytes 49160 | tf_op jit(solution)/shard_map/ppermute | solution.py:277
  68.8 11.5 %copy-start.3 = (bf16[512,256]{1,0:T(8,128)(2,1)S(1)}, bf16[512,256]{1,0:T(8,128)(2,1)}, u32[]{:S(2)}) copy-start(bf16[512,256]{1,0:T(8,128)(2,1)} %down_w.1) | copy-start | bytes 786436
